TPU v7x, 32 devices: a whole 2x2x4 slice. The times are simulated.
32 devices in a mesh: rep: 2 (over x), fs: 8 (over z, y), tp: 2 (over core).
Axes of the slice: x: 2, y: 2, z: 4, core: 2. Of those that a mesh axis runs over, the one named last changes fastest.
Arguments:
- inputs: bfloat16 [6144, 2048], P(('rep', 'fs')), may hold values from -6 to 6
- w_up: bfloat16 [2048, 4096], P('fs', 'tp'), may hold values from -0.125 to 0.125
- w_down: bfloat16 [4096, 2048], P('tp', 'fs'), may hold values from -0.09375 to 0.09375
- cotangent: bfloat16 [6144, 2048], P(('rep', 'fs')), may hold values from -6 to 6
Outputs:
- d_inputs: bfloat16 [6144, 2048], P(('rep', 'fs'))
- d_w_up: float32 [2048, 4096], P('fs', 'tp')
All inputs are finite; a program needn't handle non-finite values.
Results may differ from a plain program's by a relative error of at most 0.014.
Values may be sent and summed in bfloat16 or wider, within the bound.
A program may use at most 128 MiB of HBM per device.

v0:
```python
import functools

import jax
import jax.numpy as jnp
from jax import lax
from jax.experimental import pallas as pl
from jax.experimental.pallas import tpu as pltpu
from jax.sharding import PartitionSpec as P

MESH = pl.DeviceIdType.MESH
F32, BF16 = jnp.float32, jnp.bfloat16
CHUNKS = 2


def dot(a, b, da, db):
    return lax.dot_general(a, b, (((da,), (db,)), ((), ())), preferred_element_type=F32)


def kernel(line, n_tp, native, x_in, c_in, up_in, down_in, dw_out, din_out,
           xs, wu, wd, acc, g, dw, zin, fin, part_, tpin, q1, q2, fo,
           zs, zr, ys, yr, ts, tr, cs, cr, ls, os, orr, es, er, el, ps, pr, qs, qr, ds, dr, dl):
    r, f, c = lax.axis_index("rep"), lax.axis_index("fs"), lax.axis_index("tp")
    p, at = lax.rem(f, 2), lax.div(f, 2)
    core = lax.rem(c, 2)
    to_x, to_y = {"rep": 1 - r}, {"fs": f + 1 - 2 * p}
    to_core = {"tp": c + 1 - 2 * core}
    up, down = {"fs": f + 2}, {"fs": f - 2}
    has_up, has_down = at < line - 1, at > 0
    tokens, width = x_in.shape
    rows, cols = wu.shape[2:]
    level = 2 * rows
    quarter = 2 * r + p

    barrier = pltpu.get_barrier_semaphore()
    peers = [{"tp": lax.rem(c + k, n_tp)} for k in range(1, n_tp)]
    for dev in [to_x, to_y] + peers:
        pl.semaphore_signal(barrier, inc=1, device_id=dev, device_id_type=MESH)

    @pl.when(has_up)
    def _():
        pl.semaphore_signal(barrier, inc=1, device_id=up, device_id_type=MESH)

    @pl.when(has_down)
    def _():
        pl.semaphore_signal(barrier, inc=1, device_id=down, device_id_type=MESH)

    def remote(src, dst, send, recv, dev):
        return pltpu.make_async_remote_copy(
            src_ref=src, dst_ref=dst, send_sem=send, recv_sem=recv, device_id=dev, device_id_type=MESH
        )

    half = tokens // 2
    mine = pl.ds(pl.multiple_of(core * half, half), half)
    theirs = pl.ds(pl.multiple_of((1 - core) * half, half), half)
    ws = (wu, wd)

    def own_block(u, q):
        span = pl.ds(pl.multiple_of(q * cols, cols), cols)
        if u == 1 and native:
            return down_in.at[span, :]
        return (up_in, down_in)[u].at[:, span]

    own_x = pltpu.make_async_copy(x_in, xs.at[0, 0], ls.at[0])
    own_c = pltpu.make_async_copy(c_in, xs.at[1, 0], ls.at[1])
    own_w = [pltpu.make_async_copy(own_block(u, quarter), ws[u].at[at, p], ls.at[2 + u]) for u in (0, 1)]
    own_x.start()
    own_c.start()
    for copy in own_w:
        copy.start()
    acc[...] = jnp.zeros_like(acc)

    n_near = n_tp + 1
    inner = has_up & has_down

    @pl.when(inner)
    def _():
        pl.semaphore_wait(barrier, n_near + 2)

    @pl.when(jnp.logical_not(inner))
    def _():
        pl.semaphore_wait(barrier, n_near + 1 if line > 1 else n_near)

    y_copies = [
        remote(own_block(u, 2 * r + 1 - p), ws[u].at[at, p], ys.at[u], yr.at[u], to_y) for u in (0, 1)
    ]

    def y_arrival(u):
        blk = ws[u].at[at, 1 - p]
        return remote(blk, blk, ys.at[u], yr.at[u], to_y)

    for copy in y_copies:
        copy.start()

    def z_copy(go_up, s, j):
        u, own_pair = j % 2, j < 2
        lvl = at - s if go_up else at + s
        blk = ws[u].at[lvl, p if own_pair else 1 - p]
        src = own_block(u, quarter) if (s == 0 and own_pair) else blk
        d = 0 if go_up else 1
        return remote(src, blk, zs.at[d, s, j], zr.at[d, s, j], up if go_up else down)

    def z_valid(go_up, s):
        return ((at - s >= 0) & has_up) if go_up else ((at + s < line) & has_down)

    def z_step(s, j):
        for go_up in (True, False):
            d = 0 if go_up else 1
            if s > 0:
                lvl = at - s if go_up else at + s

                @pl.when((lvl >= 0) & (lvl < line))
                def _():
                    blk = ws[j % 2].at[lvl, p if j < 2 else 1 - p]
                    remote(blk, blk, zs.at[d, s - 1, j], zr.at[d, s - 1, j], to_x).wait_recv()
            if s < line - 1:
                @pl.when(z_valid(go_up, s))
                def _():
                    z_copy(go_up, s, j).start()

    z_step(0, 0)
    z_step(0, 1)

    own = (x_in, c_in)
    first = {}
    for slot, dev in ((1, to_x), (2, to_y)):
        for a in (0, 1):
            first[slot, a] = remote(
                own[a].at[mine], xs.at[a, slot, mine], ts.at[slot - 1, a], tr.at[slot - 1, a], dev
            )
    first[1, 0].start()
    first[2, 1].start()
    first[1, 1].start()
    first[2, 0].start()
    diag = [
        remote(xs.at[0, 1, mine], xs.at[0, 3, mine], ts.at[2, 0], tr.at[2, 0], to_y),
        remote(xs.at[1, 2, mine], xs.at[1, 3, mine], ts.at[2, 1], tr.at[2, 1], to_x),
    ]

    def swap(slot, a):
        return remote(
            xs.at[a, slot, mine], xs.at[a, slot, mine], cs.at[slot - 1, a], cr.at[slot - 1, a], to_core
        )

    def swapped(slot, a):
        blk = xs.at[a, slot, theirs]
        remote(blk, blk, cs.at[slot - 1, a], cr.at[slot - 1, a], to_core).wait_recv()

    def unit(u, slot, lvl):
        if u == 1 and native:
            total = acc[u, slot]
            for b in (0, 1):
                span = pl.ds(pl.multiple_of(lvl * level + b * rows, rows), rows)
                total = total + dot(xs[u, slot, :, span], wd[lvl, b], 1, 1)
            acc[u, slot] = total
        else:
            span = pl.ds(pl.multiple_of(lvl * level, level), level)
            acc[u, slot] += dot(xs[u, slot, :, span], ws[u][lvl].reshape(level, cols), 1, 0)

    done = [-1, -1]
    ready = [1, 1]

    def grow(u, s):
        done[u] = s
        n = ready[u]
        if s == 0:
            def body(slot, _):
                unit(u, slot, at)
                return 0

            lax.fori_loop(0, n, body, 0)
            return

        def body(i, _):
            lvl = at + s - 2 * s * lax.rem(i, 2)

            @pl.when((lvl >= 0) & (lvl < line))
            def _():
                unit(u, lax.div(i, 2), lvl)
            return 0

        lax.fori_loop(0, 2 * n, body, 0)

    order = ([0, 1, 2, 3], [0, 2, 1, 3])

    def join(slot, u):
        ready[u] += 1
        lo, hi = jnp.maximum(at - done[u], 0), jnp.minimum(at + done[u], line - 1)

        def body(lvl, _):
            unit(u, slot, lvl)
            return 0

        lax.fori_loop(lo, hi + 1, body, 0)

    own_x.wait()
    own_c.wait()
    for u in (0, 1):
        own_w[u].wait()
    for u in (0, 1):
        y_arrival(u).wait_recv()
        z_step(0, 2 + u)
    for u in (0, 1):
        grow(u, 0)

    def got(slot, a):
        def run():
            if slot < 3:
                first[slot, a].wait_recv()
                if (slot, a) == (1, 0):
                    diag[0].start()
                if (slot, a) == (2, 1):
                    diag[1].start()
            else:
                diag[a].wait_recv()
            swap(slot, a).start()
        return run

    def use(slot, a):
        def run():
            swapped(slot, a)
            join(slot, a)
        return run

    hooks = {
        (1, 2): [got(1, 0)],
        (1, 3): [use(1, 0)],
        (2, 0): [got(2, 1)],
        (2, 1): [got(1, 1), use(2, 1)],
        (2, 2): [use(1, 1)],
        (2, 3): [got(2, 0)],
        (3, 0): [use(2, 0), got(3, 1)],
        (3, 1): [use(3, 1)],
        (3, 2): [got(3, 0)],
    }
    last = [use(3, 0)]
    for s in range(1, line):
        for j in range(4):
            z_step(s, j)
            if j >= 2:
                grow(j - 2, s)
            for run in hooks.pop((s, j), []):
                run()
    for key in sorted(hooks):
        for run in hooks[key]:
            run()
    for run in last:
        run()

    def make_g(slot, _):
        g[slot] = (2.0 * jnp.maximum(acc[0, slot], 0.0) * acc[1, slot]).astype(BF16)
        return 0

    lax.fori_loop(0, 4, make_g, 0)

    low = at < line - at - 1
    sub = rows // CHUNKS

    def chunk(ch):
        return pl.ds(ch * sub, sub)

    def o_copy(go_up, o, ch):
        d = 0 if go_up else 1
        return remote(
            dw.at[o, :, chunk(ch)], zin.at[d, o, :, chunk(ch)],
            os.at[d, o, ch], orr.at[d, o, ch], up if go_up else down,
        )

    def make_dw(i):
        o = jnp.where(low, line - 1 - i, i)
        span = pl.ds(pl.multiple_of(o * level, level), level)
        lhs = xs[0, :, :, span].reshape(4 * tokens, level)
        value = dot(lhs, g[...].reshape(4 * tokens, cols), 0, 0)
        dw[o] = value.astype(BF16).reshape(2, rows, cols)

    def send_ends(i, ch):
        @pl.when((at == 0) & (line > 1))
        def _():
            o_copy(True, line - 1 - i, ch).start()

        @pl.when((at == line - 1) & (line > 1))
        def _():
            o_copy(False, i, ch).start()

    def p_copy(slot, k):
        there = lax.rem(c + k, n_tp)
        return remote(
            part_.at[slot, there], tpin.at[k - 1, slot], ps.at[k - 1, slot], pr.at[k - 1, slot], {"tp": there}
        )

    part = tokens // n_tp

    def make_part(slot):
        def body(lvl, _):
            span = pl.ds(pl.multiple_of(lvl * level, level), level)
            value = dot(g[slot], wu[lvl].reshape(level, cols), 1, 1)
            part_[slot, :, :, span] = value.astype(BF16).reshape(n_tp, part, level)
            return 0

        lax.fori_loop(0, line, body, 0)
        for k in range(1, n_tp):
            p_copy(slot, k).start()

    def tp_sum(slot):
        for k in range(1, n_tp):
            p_copy(slot, k).wait_recv()
        total = part_[slot, c].astype(F32)
        for k in range(1, n_tp):
            total = total + tpin[k - 1, slot].astype(F32)
        return total

    cut = (width * 3 // 8) // 128 * 128
    left, right = pl.ds(0, cut), pl.ds(cut, width - cut)
    q_copies = {
        "x3": remote(part_.at[3, c, :, left], q1.at[1, :, left], qs.at[0], qr.at[0], to_x),
        "y3": remote(part_.at[3, c, :, right], q1.at[1, :, right], qs.at[1], qr.at[1], to_y),
        "x1": remote(part_.at[1, c, :, left], q1.at[0, :, left], qs.at[2], qr.at[2], to_x),
        "y2": remote(part_.at[2, c, :, right], q1.at[0, :, right], qs.at[3], qr.at[3], to_y),
        "y2r": remote(part_.at[2, c, :, left], q2.at[:, left], qs.at[4], qr.at[4], to_y),
        "x1r": remote(part_.at[1, c, :, right], q2.at[:, right], qs.at[5], qr.at[5], to_x),
    }

    def store_sum(slot):
        part_[slot, c] = tp_sum(slot).astype(BF16)

    make_dw(0)
    send_ends(0, 0)
    make_part(3)
    make_part(1)
    make_part(2)
    store_sum(3)
    q_copies["x3"].start()
    q_copies["y3"].start()
    if line > 2:
        make_dw(1)
        send_ends(1, 0)
    store_sum(1)
    q_copies["x1"].start()
    store_sum(2)
    q_copies["y2"].start()
    for i in range(2, line - 1):
        make_dw(i)
        send_ends(i, 0)
    for ch in range(1, CHUNKS):
        for i in range(line - 1):
            send_ends(i, ch)
    if line > 1:
        make_dw(line - 1)
    make_part(0)

    def add_in(d, o, ch):
        dw[o, :, chunk(ch)] = (
            dw[o, :, chunk(ch)].astype(F32) + zin[d, o, :, chunk(ch)].astype(F32)
        ).astype(BF16)

    def o_step(t, ch):
        for go_up in (True, False):
            d = 0 if go_up else 1
            gap = at if go_up else line - 1 - at
            o = (line - 1 - t + at) if go_up else (t - line + 1 + at)

            @pl.when((gap > 0) & (gap <= t))
            def _():
                o_copy(go_up, o, ch).wait_recv()
                if t < line - 1:
                    add_in(d, o, ch)
                    o_copy(go_up, o, ch).start()

    def rows_of(ch):
        return pl.ds(ch * sub, sub)

    e_x = [remote(fin.at[ch, p], dw_out.at[quarter, rows_of(ch)], es.at[0, ch], er.at[0, ch], to_x) for ch in range(CHUNKS)]
    e_y = [remote(fin.at[ch, 1 - p], dw_out.at[quarter, rows_of(ch)], es.at[1, ch], er.at[1, ch], to_y) for ch in range(CHUNKS)]
    e_own = [pltpu.make_async_copy(fin.at[ch, p], dw_out.at[quarter, rows_of(ch)], el.at[ch]) for ch in range(CHUNKS)]
    e_r = []
    for ch in range(CHUNKS):
        blk = dw_out.at[2 * r + 1 - p, rows_of(ch)]
        e_r.append(remote(blk, blk, es.at[2, ch], er.at[2, ch], to_x))

    def finish(ch):
        fin[ch] = dw[at, :, chunk(ch)]

        for d, there in ((0, has_down), (1, has_up)):
            if line > 2:
                @pl.when(there & jnp.logical_not(has_up & has_down))
                def _():
                    fin[ch] = (dw[at, :, chunk(ch)].astype(F32) + zin[d, at, :, chunk(ch)].astype(F32)).astype(BF16)
            elif line == 2:
                @pl.when(there)
                def _():
                    fin[ch] = (dw[at, :, chunk(ch)].astype(F32) + zin[d, at, :, chunk(ch)].astype(F32)).astype(BF16)

        @pl.when(has_up & has_down)
        def _():
            fin[ch] = (
                dw[at, :, chunk(ch)].astype(F32)
                + zin[0, at, :, chunk(ch)].astype(F32)
                + zin[1, at, :, chunk(ch)].astype(F32)
            ).astype(BF16)

        e_x[ch].start()
        e_y[ch].start()
        e_own[ch].start()

    def relay(ch):
        blk = dw_out.at[2 * r + 1 - p, rows_of(ch)]
        remote(blk, blk, es.at[1, ch], er.at[1, ch], to_y).wait_recv()
        e_r[ch].start()

    def in_first():
        q_copies["x3"].wait_recv()
        part_[2, c, :, left] = (part_[2, c, :, left].astype(F32) + q1[1, :, left].astype(F32)).astype(BF16)
        q_copies["y2r"].start()
        q_copies["y3"].wait_recv()
        part_[1, c, :, right] = (part_[1, c, :, right].astype(F32) + q1[1, :, right].astype(F32)).astype(BF16)
        q_copies["x1r"].start()

    out_own = pltpu.make_async_copy(fo, din_out.at[c], dl.at[0])
    out_peers = [
        remote(fo, din_out.at[c], ds.at[k - 1], dr.at[k - 1], {"tp": lax.rem(c + k, n_tp)}) for k in range(1, n_tp)
    ]

    def in_last():
        total = tp_sum(0)
        for name in ("x1", "y2", "y2r", "x1r"):
            q_copies[name].wait_recv()
        fo[...] = (total + q1[0].astype(F32) + q2[...].astype(F32)).astype(BF16)
        out_own.start()
        for copy in out_peers:
            copy.start()

    late = {(0, min(2, line - 1)): [in_first], (CHUNKS - 1, min(2, line - 1)): [in_last]}
    for ch in range(CHUNKS):
        for t in range(1, line):
            o_step(t, ch)
            if t == line - 1:
                finish(ch)
            for run in late.pop((ch, t), []):
                run()
            if ch > 0 and t == 1:
                relay(ch - 1)
        if line == 1:
            finish(ch)
            if ch > 0:
                relay(ch - 1)
    for key in sorted(late):
        for run in late[key]:
            run()
    relay(CHUNKS - 1)

    for k in range(1, n_tp):
        out_peers[k - 1].wait_recv()
    for ch in range(CHUNKS):
        for q, col in ((2 * (1 - r) + p, 0), (2 * (1 - r) + 1 - p, 2)):
            blk = dw_out.at[q, rows_of(ch)]
            remote(blk, blk, es.at[col, ch], er.at[col, ch], to_x).wait_recv()
    out_own.wait()
    for copy in e_own:
        copy.wait()
    for copy in out_peers + e_x + e_y + e_r + list(q_copies.values()):
        copy.wait_send()
    for slot in range(4):
        for k in range(1, n_tp):
            p_copy(slot, k).wait_send()
    for ch in range(CHUNKS):
        for o in range(line):
            @pl.when((at < o) & has_up)
            def _():
                o_copy(True, o, ch).wait_send()

            @pl.when((at > o) & has_down)
            def _():
                o_copy(False, o, ch).wait_send()
    for slot in (1, 2, 3):
        for a in (0, 1):
            swap(slot, a).wait_send()
    for copy in list(first.values()) + diag + y_copies:
        copy.wait_send()
    for s in range(line - 1):
        for j in range(4):
            for go_up in (True, False):
                @pl.when(z_valid(go_up, s))
                def _():
                    z_copy(go_up, s, j).wait_send()


def fused(n_fs, n_tp, n_rep, x, c, w_up, w_down):
    line = n_fs // 2
    tokens, width = x.shape
    rows, block = w_up.shape
    cols = block // (2 * n_rep)
    native = rows % 128 == 0
    if not native:
        w_down = w_down.T
    part = tokens // n_tp
    dma = pltpu.SemaphoreType.DMA
    hbm = pl.BlockSpec(memory_space=pl.ANY)
    vmem = lambda *shape: pltpu.VMEM(shape, BF16)
    down_block = (cols, rows) if native else (rows, cols)
    others = max(n_tp - 1, 1)
    return pl.pallas_call(
        functools.partial(kernel, line, n_tp, native),
        out_shape=(
            jax.ShapeDtypeStruct((2 * n_rep, rows, cols), BF16),
            jax.ShapeDtypeStruct((n_tp, part, width), BF16),
        ),
        in_specs=[hbm] * 4,
        out_specs=(hbm,) * 2,
        scratch_shapes=[
            vmem(2, 4, tokens, width),
            vmem(line, 2, rows, cols),
            vmem(line, 2, *down_block),
            pltpu.VMEM((2, 4, tokens, cols), F32),
            vmem(4, tokens, cols),
            vmem(line, 2, rows, cols),
            vmem(2, line, 2, rows, cols),
            vmem(CHUNKS, 2, rows // CHUNKS, cols),
            vmem(4, n_tp, part, width),
            vmem(others, 4, part, width),
            vmem(2, part, width),
            vmem(part, width),
            vmem(part, width),
            dma((2, line, 4)), dma((2, line, 4)), dma((2,)), dma((2,)),
            dma((3, 2)), dma((3, 2)), dma((3, 2)), dma((3, 2)), dma((4,)),
            dma((2, line, CHUNKS)), dma((2, line, CHUNKS)),
            dma((3, CHUNKS)), dma((3, CHUNKS)), dma((CHUNKS,)),
            dma((others, 4)), dma((others, 4)), dma((6,)), dma((6,)),
            dma((others,)), dma((others,)), dma((1,)),
        ],
        compiler_params=pltpu.CompilerParams(
            collective_id=0, has_side_effects=True, vmem_limit_bytes=60 * 2**20
        ),
        name="fused",
    )(x, c, w_up, w_down)


def per_device(inputs, w_up, w_down, cotangent):
    n_rep, n_fs, n_tp = lax.axis_size("rep"), lax.axis_size("fs"), lax.axis_size("tp")
    rows, block = w_up.shape
    d_w, d_in = fused(n_fs, n_tp, n_rep, inputs, cotangent, w_up, w_down)
    d_w_up = d_w.transpose(1, 0, 2).reshape(rows, block).astype(F32)
    return d_in.reshape(inputs.shape), d_w_up


def solution(mesh):
    in_specs = (P(("rep", "fs"), None), P("fs", "tp"), P("tp", "fs"), P(("rep", "fs"), None))
    out_specs = (P(("rep", "fs"), None), P("fs", "tp"))
    return jax.shard_map(
        per_device, mesh=mesh, in_specs=in_specs, out_specs=out_specs, check_vma=False
    )
```

profile of v0, /device:TPU:0, one launch (start us, length us, event | category | flops | bytes accessed | tf_op | source)
XLA Modules:
  0.0 136.0 jit_solution(4193629286274003230)
XLA Ops:
  0.6 127.8 %fused.1 = (bf16[4,256,512]{2,1,0:T(8,128)(2,1)}, bf16[2,192,2048]{2,1,0:T(8,128)(2,1)}) custom-call(bf16[384,2048]{1,0:T(8,128)(2,1)} %x_in.1, bf16[384,2048]{1,0:T(8,128)(2,1)} %c_in.1, bf16[256,2048]{1,0:T(8,128)(2,1)} %up_in.1, bf16[2048,256]{1,0:T(8,128)(2,1)} %down_in.1), custom_call_target="tpu_custom_call" | custom-call | tf_op jit(solution)/shard_map/fused/pallas_call | solution.py:500
  128.5 1.5 %convert_bitcast_fusion = f32[256,4,512]{2,0,1:T(8,128)S(1)} fusion(bf16[4,256,512]{2,1,0:T(8,128)(2,1)} %get-tuple-element.5), kind=kLoop, calls=%fused_computation | loop fusion | flops 524288 | bytes 3145728 | tf_op jit(solution)/shard_map/convert_element_type | solution.py:540
  130.0 1.9 %copy.6 = f32[256,4,512]{0,2,1:T(8,128)} copy(f32[256,4,512]{2,0,1:T(8,128)S(1)} %convert_bitcast_fusion) | data formatting | bytes 4194304 | tf_op jit(solution)/shard_map/convert_element_type | solution.py:540
  131.8 0.0 copy-start
  131.8 3.0 %copy.7 = f32[256,2048]{1,0:T(8,128)} copy(f32[256,2048]{0,1:T(8,128)} %bitcast.4) | data formatting | bytes 4194304
  134.8 0.0 copy-done
  134.8 1.1 copy.9
Async XLA Ops:
  131.8 3.0 %copy-start = (bf16[2,192,2048]{2,1,0:T(8,128)(2,1)S(1)}, bf16[2,192,2048]{2,1,0:T(8,128)(2,1)}, u32[]{:S(2)}) copy-start(bf16[2,192,2048]{2,1,0:T(8,128)(2,1)} %get-tuple-element.4) | copy-start | bytes 4718596
where the time goes:
time: 136 us
  Pallas kernels  128 us (94%)
  local copies, waits for them, and re-layouts  6.01 us (4%)
  other arithmetic  1.5 us (1%)
    pallas_call x1, Pallas kernels, fused(): pl.pallas_call(functools.partial(kernel, line, n_tp, native), out_shape=(...  128 us
    unnamed x4, local copies, waits for them, and re-layouts  4.14 us

commit v1 on v0

v1 whole, which is shorter than its diff:
```python
import functools

import jax
import jax.numpy as jnp
from jax import lax
from jax.experimental import pallas as pl
from jax.experimental.pallas import tpu as pltpu
from jax.sharding import PartitionSpec as P

MESH = pl.DeviceIdType.MESH
F32, BF16 = jnp.float32, jnp.bfloat16


def dot(a, b, da, db):
    return lax.dot_general(a, b, (((da,), (db,)), ((), ())), preferred_element_type=F32)


def kernel(line, n_tp, native, parts, x_in, c_in, up_in, down_in, dw_out, din_out,
           xs, wu, wd, acc, g, dw, zin, fin, part_, tpin, q1, q2, fo,
           zs, zr, ys, yr, ts, tr, cs, cr, ls, os, orr, es, er, el, ps, pr, qs, qr, ds, dr, dl):
    r, f, c = lax.axis_index("rep"), lax.axis_index("fs"), lax.axis_index("tp")
    p, at = lax.rem(f, 2), lax.div(f, 2)
    core = lax.rem(c, 2)
    to_x, to_y = {"rep": 1 - r}, {"fs": f + 1 - 2 * p}
    to_core = {"tp": c + 1 - 2 * core}
    up, down = {"fs": f + 2}, {"fs": f - 2}
    has_up, has_down = at < line - 1, at > 0
    tokens, width = x_in.shape
    rows, cols = wu.shape[3:]
    level = 2 * rows
    final = parts - 1
    quarter = 2 * r + p

    barrier = pltpu.get_barrier_semaphore()
    peers = [{"tp": lax.rem(c + k, n_tp)} for k in range(1, n_tp)]
    for dev in [to_x, to_y] + peers:
        pl.semaphore_signal(barrier, inc=1, device_id=dev, device_id_type=MESH)

    @pl.when(has_up)
    def _():
        pl.semaphore_signal(barrier, inc=1, device_id=up, device_id_type=MESH)

    @pl.when(has_down)
    def _():
        pl.semaphore_signal(barrier, inc=1, device_id=down, device_id_type=MESH)

    def remote(src, dst, send, recv, dev):
        return pltpu.make_async_remote_copy(
            src_ref=src, dst_ref=dst, send_sem=send, recv_sem=recv, device_id=dev, device_id_type=MESH
        )

    half = tokens // 2
    mine = pl.ds(pl.multiple_of(core * half, half), half)
    theirs = pl.ds(pl.multiple_of((1 - core) * half, half), half)
    ws = (wu, wd)

    def own_block(u, q, h):
        span = pl.ds(pl.multiple_of((q * parts + h) * cols, cols), cols)
        if u == 1 and native:
            return down_in.at[span, :]
        return (up_in, down_in)[u].at[:, span]

    own_x = pltpu.make_async_copy(x_in, xs.at[0, 0], ls.at[0])
    own_c = pltpu.make_async_copy(c_in, xs.at[1, 0], ls.at[1])
    own_w = [
        pltpu.make_async_copy(own_block(u, quarter, h), ws[u].at[h, at, p], ls.at[2 + 2 * h + u])
        for h in range(parts) for u in (0, 1)
    ]
    own_x.start()
    own_c.start()
    for copy in own_w:
        copy.start()
    acc[...] = jnp.zeros_like(acc)

    n_near = n_tp + 1
    inner = has_up & has_down

    @pl.when(inner)
    def _():
        pl.semaphore_wait(barrier, n_near + 2)

    @pl.when(jnp.logical_not(inner))
    def _():
        pl.semaphore_wait(barrier, n_near + 1 if line > 1 else n_near)

    y_copies = [
        remote(own_block(u, 2 * r + 1 - p, h), ws[u].at[h, at, p], ys.at[h, u], yr.at[h, u], to_y)
        for h in range(parts) for u in (0, 1)
    ]

    def y_arrival(u, h):
        blk = ws[u].at[h, at, 1 - p]
        return remote(blk, blk, ys.at[h, u], yr.at[h, u], to_y)

    for copy in y_copies:
        copy.start()

    def z_copy(go_up, h, s, j):
        u, own_pair = j % 2, j < 2
        lvl = at - s if go_up else at + s
        blk = ws[u].at[h, lvl, p if own_pair else 1 - p]
        src = own_block(u, quarter, h) if (s == 0 and own_pair) else blk
        d = 0 if go_up else 1
        return remote(src, blk, zs.at[d, h, s, j], zr.at[d, h, s, j], up if go_up else down)

    def z_valid(go_up, s):
        return ((at - s >= 0) & has_up) if go_up else ((at + s < line) & has_down)

    def z_step(h, s, j):
        for go_up in (True, False):
            d = 0 if go_up else 1
            if s > 0:
                lvl = at - s if go_up else at + s

                @pl.when((lvl >= 0) & (lvl < line))
                def _():
                    blk = ws[j % 2].at[h, lvl, p if j < 2 else 1 - p]
                    remote(blk, blk, zs.at[d, h, s - 1, j], zr.at[d, h, s - 1, j], to_x).wait_recv()
            if s < line - 1:
                @pl.when(z_valid(go_up, s))
                def _():
                    z_copy(go_up, h, s, j).start()

    z_step(0, 0, 0)
    z_step(0, 0, 1)

    own = (x_in, c_in)
    first = {}
    for slot, dev in ((1, to_x), (2, to_y)):
        for a in (0, 1):
            first[slot, a] = remote(
                own[a].at[mine], xs.at[a, slot, mine], ts.at[slot - 1, a], tr.at[slot - 1, a], dev
            )
    first[1, 0].start()
    first[2, 1].start()
    first[1, 1].start()
    first[2, 0].start()
    diag = [
        remote(xs.at[0, 1, mine], xs.at[0, 3, mine], ts.at[2, 0], tr.at[2, 0], to_y),
        remote(xs.at[1, 2, mine], xs.at[1, 3, mine], ts.at[2, 1], tr.at[2, 1], to_x),
    ]

    def swap(slot, a):
        return remote(
            xs.at[a, slot, mine], xs.at[a, slot, mine], cs.at[slot - 1, a], cr.at[slot - 1, a], to_core
        )

    def swapped(slot, a):
        blk = xs.at[a, slot, theirs]
        remote(blk, blk, cs.at[slot - 1, a], cr.at[slot - 1, a], to_core).wait_recv()

    def unit(u, h, slot, lvl):
        if u == 1 and native:
            total = acc[h, u, slot]
            for b in (0, 1):
                span = pl.ds(pl.multiple_of(lvl * level + b * rows, rows), rows)
                total = total + dot(xs[u, slot, :, span], wd[h, lvl, b], 1, 1)
            acc[h, u, slot] = total
        else:
            span = pl.ds(pl.multiple_of(lvl * level, level), level)
            acc[h, u, slot] += dot(xs[u, slot, :, span], ws[u][h, lvl].reshape(level, cols), 1, 0)

    done = [[-1, -1] for _ in range(parts)]
    ready = [1, 1]

    def grow_slot(u, h, s, slot):
        for lvl in (at - s, at + s):
            @pl.when((lvl >= 0) & (lvl < line))
            def _():
                unit(u, h, slot, lvl)

    def grow(u, h, s):
        done[h][u] = s
        n = ready[u]
        if s == 0:
            def body(slot, _):
                unit(u, h, slot, at)
                return 0

            lax.fori_loop(0, n, body, 0)
            return

        def body(i, _):
            lvl = at + s - 2 * s * lax.rem(i, 2)

            @pl.when((lvl >= 0) & (lvl < line))
            def _():
                unit(u, h, lax.div(i, 2), lvl)
            return 0

        lax.fori_loop(0, 2 * n, body, 0)

    def join(slot, u):
        ready[u] += 1
        for h in range(parts):
            lo, hi = jnp.maximum(at - done[h][u], 0), jnp.minimum(at + done[h][u], line - 1)

            def body(lvl, _):
                unit(u, h, slot, lvl)
                return 0

            lax.fori_loop(lo, hi + 1, body, 0)

    def make_g(h, slot):
        g[h, slot] = (2.0 * jnp.maximum(acc[h, 0, slot], 0.0) * acc[h, 1, slot]).astype(BF16)

    low = at < line - at - 1

    def o_copy(go_up, h, o):
        d = 0 if go_up else 1
        return remote(dw.at[h, o], zin.at[d, h, o], os.at[d, h, o], orr.at[d, h, o], up if go_up else down)

    def make_dw(h, i):
        o = jnp.where(low, line - 1 - i, i)
        span = pl.ds(pl.multiple_of(o * level, level), level)
        lhs = xs[0, :, :, span].reshape(4 * tokens, level)
        value = dot(lhs, g[h].reshape(4 * tokens, cols), 0, 0)
        dw[h, o] = value.astype(BF16).reshape(2, rows, cols)
        if i < line - 1:
            @pl.when(at == 0)
            def _():
                o_copy(True, h, line - 1 - i).start()

            @pl.when(at == line - 1)
            def _():
                o_copy(False, h, i).start()

    own_x.wait()
    own_c.wait()
    for copy in own_w:
        copy.wait()

    def own_level(h):
        for u in (0, 1):
            y_arrival(u, h).wait_recv()
            z_step(h, 0, 2 + u)
        for u in (0, 1):
            grow(u, h, 0)

    own_level(0)

    def got(slot, a):
        def run():
            if slot < 3:
                first[slot, a].wait_recv()
                if (slot, a) == (1, 0):
                    diag[0].start()
                if (slot, a) == (2, 1):
                    diag[1].start()
            else:
                diag[a].wait_recv()
            swap(slot, a).start()
        return run

    def use(slot, a):
        def run():
            swapped(slot, a)
            join(slot, a)
        return run

    def early():
        for h in range(final):
            def body(slot, _):
                make_g(h, slot)
                return 0

            lax.fori_loop(0, 4, body, 0)
            for i in range(line):
                make_dw(h, i)

    if parts == 2:
        hooks = {
            (0, 2, 1): [got(1, 0)],
            (0, 2, 3): [use(1, 0)],
            (1, 1, 1): [got(2, 1)],
            (1, 1, 3): [use(2, 1), got(1, 1)],
            (0, 3, 0): [use(1, 1)],
            (0, 3, 3): [got(2, 0)],
            (1, 2, 0): [use(2, 0)],
            (1, 2, 1): [got(3, 1)],
            (1, 2, 2): [use(3, 1)],
            (1, 3, 1): [got(3, 0)],
            (1, 3, 2): [use(3, 0), early],
        }
        steps = [(0, 1)]
        for s in range(2, line):
            steps += [(0, s), (1, s - 1)]
        steps += [(1, line - 1)]
    else:
        hooks = {
            (0, 1, 2): [got(1, 0)],
            (0, 1, 3): [use(1, 0)],
            (0, 2, 0): [got(2, 1)],
            (0, 2, 1): [got(1, 1), use(2, 1)],
            (0, 2, 2): [use(1, 1)],
            (0, 2, 3): [got(2, 0)],
            (0, 3, 0): [use(2, 0), got(3, 1)],
            (0, 3, 1): [use(3, 1)],
            (0, 3, 2): [got(3, 0)],
            (0, 3, 3): [use(3, 0), early],
        }
        steps = [(0, s) for s in range(1, line)]
    for h, s in steps:
        for j in range(4):
            z_step(h, s, j)
            if j >= 2 and (h, s, j) != (final, line - 1, 3):
                grow(j - 2, h, s)
            for run in hooks.pop((h, s, j), []):
                run()
        if (h, s) == (0, 1):
            for k in range(1, parts):
                z_step(k, 0, 0)
                z_step(k, 0, 1)
                own_level(k)
    for key in list(hooks):
        for run in hooks[key]:
            run()

    def p_copy(slot, k):
        there = lax.rem(c + k, n_tp)
        return remote(
            part_.at[slot, there], tpin.at[k - 1, slot], ps.at[k - 1, slot], pr.at[k - 1, slot], {"tp": there}
        )

    part = tokens // n_tp

    def make_part(slot):
        def body(lvl, _):
            span = pl.ds(pl.multiple_of(lvl * level, level), level)
            value = dot(g[0, slot], wu[0, lvl].reshape(level, cols), 1, 1)
            for h in range(1, parts):
                value = value + dot(g[h, slot], wu[h, lvl].reshape(level, cols), 1, 1)
            part_[slot, :, :, span] = value.astype(BF16).reshape(n_tp, part, level)
            return 0

        lax.fori_loop(0, line, body, 0)
        for k in range(1, n_tp):
            p_copy(slot, k).start()

    def tp_sum(slot):
        for k in range(1, n_tp):
            p_copy(slot, k).wait_recv()
        total = part_[slot, c].astype(F32)
        for k in range(1, n_tp):
            total = total + tpin[k - 1, slot].astype(F32)
        return total

    cut = (width * 3 // 8) // 128 * 128
    left, right = pl.ds(0, cut), pl.ds(cut, width - cut)
    q_copies = {
        "x3": remote(part_.at[3, c, :, left], q1.at[1, :, left], qs.at[0], qr.at[0], to_x),
        "y3": remote(part_.at[3, c, :, right], q1.at[1, :, right], qs.at[1], qr.at[1], to_y),
        "x1": remote(part_.at[1, c, :, left], q1.at[0, :, left], qs.at[2], qr.at[2], to_x),
        "y2": remote(part_.at[2, c, :, right], q1.at[0, :, right], qs.at[3], qr.at[3], to_y),
        "y2r": remote(part_.at[2, c, :, left], q2.at[:, left], qs.at[4], qr.at[4], to_y),
        "x1r": remote(part_.at[1, c, :, right], q2.at[:, right], qs.at[5], qr.at[5], to_x),
    }

    def store_sum(slot):
        part_[slot, c] = tp_sum(slot).astype(BF16)

    def add_in(d, h, o):
        dw[h, o] = (dw[h, o].astype(F32) + zin[d, h, o].astype(F32)).astype(BF16)

    def o_step(h, t):
        for go_up in (True, False):
            d = 0 if go_up else 1
            gap = at if go_up else line - 1 - at
            o = (line - 1 - t + at) if go_up else (t - line + 1 + at)

            @pl.when((gap > 0) & (gap <= t))
            def _():
                o_copy(go_up, h, o).wait_recv()
                if t < line - 1:
                    add_in(d, h, o)
                    o_copy(go_up, h, o).start()

    def dw_at(q, h):
        return dw_out.at[:, pl.ds(pl.multiple_of((q * parts + h) * cols, cols), cols)]

    e_x, e_y, e_own, e_r = [], [], [], []
    for h in range(parts):
        here, across = dw_at(quarter, h), dw_at(2 * r + 1 - p, h)
        e_x.append(remote(fin.at[h, p], here, es.at[0, h], er.at[0, h], to_x))
        e_y.append(remote(fin.at[h, 1 - p], here, es.at[1, h], er.at[1, h], to_y))
        e_own.append(pltpu.make_async_copy(fin.at[h, p], here, el.at[h]))
        e_r.append(remote(across, across, es.at[2, h], er.at[2, h], to_x))

    def finish(h):
        if line == 1:
            fin[h] = dw[h, at]
        for d, there in ((0, has_down), (1, has_up)):
            if line > 1:
                @pl.when(there & jnp.logical_not(has_up & has_down))
                def _():
                    fin[h] = (dw[h, at].astype(F32) + zin[d, h, at].astype(F32)).astype(BF16)

        @pl.when(has_up & has_down)
        def _():
            total = dw[h, at].astype(F32) + zin[0, h, at].astype(F32) + zin[1, h, at].astype(F32)
            fin[h] = total.astype(BF16)

        e_x[h].start()
        e_y[h].start()
        e_own[h].start()

    def relay(h):
        blk = dw_at(2 * r + 1 - p, h)
        remote(blk, blk, es.at[1, h], er.at[1, h], to_y).wait_recv()
        e_r[h].start()

    def in_first():
        q_copies["x3"].wait_recv()
        part_[2, c, :, left] = (part_[2, c, :, left].astype(F32) + q1[1, :, left].astype(F32)).astype(BF16)
        q_copies["y2r"].start()
        q_copies["y3"].wait_recv()
        part_[1, c, :, right] = (part_[1, c, :, right].astype(F32) + q1[1, :, right].astype(F32)).astype(BF16)
        q_copies["x1r"].start()

    out_own = pltpu.make_async_copy(fo, din_out.at[c], dl.at[0])
    out_peers = [
        remote(fo, din_out.at[c], ds.at[k - 1], dr.at[k - 1], {"tp": lax.rem(c + k, n_tp)}) for k in range(1, n_tp)
    ]

    def in_last():
        total = tp_sum(0)
        for name in ("x1", "y2", "y2r", "x1r"):
            q_copies[name].wait_recv()
        fo[...] = (total + q1[0].astype(F32) + q2[...].astype(F32)).astype(BF16)
        out_own.start()
        for copy in out_peers:
            copy.start()

    def last_rows(slot):
        if line > 1:
            grow_slot(1, final, line - 1, slot)
        make_g(final, slot)
        make_part(slot)

    last_rows(3)
    last_rows(1)
    store_sum(3)
    q_copies["x3"].start()
    q_copies["y3"].start()
    if parts > 1:
        o_step(0, 1)
    last_rows(2)
    store_sum(1)
    q_copies["x1"].start()
    store_sum(2)
    q_copies["y2"].start()
    last_rows(0)
    for i in range(line):
        make_dw(final, i)
    if parts == 1 and line > 1:
        o_step(0, 1)
    for t in range(2, line - 1):
        o_step(0, t)
    in_first()
    if line > 2:
        o_step(0, line - 1)
    finish(0)
    for h in range(1, parts):
        for t in range(1, line):
            o_step(h, t)
            if t == 1:
                relay(h - 1)
        if line == 1:
            relay(h - 1)
        finish(h)
    in_last()
    relay(final)

    for k in range(1, n_tp):
        out_peers[k - 1].wait_recv()
    for h in range(parts):
        for q, col in ((2 * (1 - r) + p, 0), (2 * (1 - r) + 1 - p, 2)):
            blk = dw_at(q, h)
            remote(blk, blk, es.at[col, h], er.at[col, h], to_x).wait_recv()
    out_own.wait()
    for copy in e_own:
        copy.wait()
    for copy in out_peers + e_x + e_y + e_r + list(q_copies.values()):
        copy.wait_send()
    for slot in range(4):
        for k in range(1, n_tp):
            p_copy(slot, k).wait_send()
    for h in range(parts):
        for o in range(line):
            @pl.when((at < o) & has_up)
            def _():
                o_copy(True, h, o).wait_send()

            @pl.when((at > o) & has_down)
            def _():
                o_copy(False, h, o).wait_send()
    for slot in (1, 2, 3):
        for a in (0, 1):
            swap(slot, a).wait_send()
    for copy in list(first.values()) + diag + y_copies:
        copy.wait_send()
    for h in range(parts):
        for s in range(line - 1):
            for j in range(4):
                for go_up in (True, False):
                    @pl.when(z_valid(go_up, s))
                    def _():
                        z_copy(go_up, h, s, j).wait_send()


def fused(n_fs, n_tp, n_rep, x, c, w_up, w_down):
    line = n_fs // 2
    tokens, width = x.shape
    rows, block = w_up.shape
    cols = block // (2 * n_rep)
    parts = 2 if cols % 256 == 0 and n_fs > 4 else 1
    cols = cols // parts
    native = rows % 128 == 0
    if not native:
        w_down = w_down.T
    part = tokens // n_tp
    dma = pltpu.SemaphoreType.DMA
    hbm = pl.BlockSpec(memory_space=pl.ANY)
    vmem = lambda *shape: pltpu.VMEM(shape, BF16)
    down_block = (cols, rows) if native else (rows, cols)
    others = max(n_tp - 1, 1)
    return pl.pallas_call(
        functools.partial(kernel, line, n_tp, native, parts),
        out_shape=(
            jax.ShapeDtypeStruct((rows, block), BF16),
            jax.ShapeDtypeStruct((n_tp, part, width), BF16),
        ),
        in_specs=[hbm] * 4,
        out_specs=(hbm,) * 2,
        scratch_shapes=[
            vmem(2, 4, tokens, width),
            vmem(parts, line, 2, rows, cols),
            vmem(parts, line, 2, *down_block),
            pltpu.VMEM((parts, 2, 4, tokens, cols), F32),
            vmem(parts, 4, tokens, cols),
            vmem(parts, line, 2, rows, cols),
            vmem(2, parts, line, 2, rows, cols),
            vmem(parts, 2, rows, cols),
            vmem(4, n_tp, part, width),
            vmem(others, 4, part, width),
            vmem(2, part, width),
            vmem(part, width),
            vmem(part, width),
            dma((2, parts, line, 4)), dma((2, parts, line, 4)), dma((parts, 2)), dma((parts, 2)),
            dma((3, 2)), dma((3, 2)), dma((3, 2)), dma((3, 2)), dma((2 + 2 * parts,)),
            dma((2, parts, line)), dma((2, parts, line)),
            dma((3, parts)), dma((3, parts)), dma((parts,)),
            dma((others, 4)), dma((others, 4)), dma((6,)), dma((6,)),
            dma((others,)), dma((others,)), dma((1,)),
        ],
        compiler_params=pltpu.CompilerParams(
            collective_id=0, has_side_effects=True, vmem_limit_bytes=60 * 2**20
        ),
        name="fused",
    )(x, c, w_up, w_down)


def per_device(inputs, w_up, w_down, cotangent):
    n_rep, n_fs, n_tp = lax.axis_size("rep"), lax.axis_size("fs"), lax.axis_size("tp")
    d_w, d_in = fused(n_fs, n_tp, n_rep, inputs, cotangent, w_up, w_down)
    return d_in.reshape(inputs.shape), d_w.astype(F32)


def solution(mesh):
    in_specs = (P(("rep", "fs"), None), P("fs", "tp"), P("tp", "fs"), P(("rep", "fs"), None))
    out_specs = (P(("rep", "fs"), None), P("fs", "tp"))
    return jax.shard_map(
        per_device, mesh=mesh, in_specs=in_specs, out_specs=out_specs, check_vma=False
    )
```

time: 136 us -> 135 us (level)
  local copies, waits for them, and re-layouts: 6.01 us -> 1.15 us
  Pallas kernels: 128 us -> 130 us
  other arithmetic: 1.5 us -> 2.91 us
    unnamed x4 -> x3, local copies, waits for them, and re-layouts: 4.14 us -> 1.15 us
    pallas_call x1, Pallas kernels: 128 us -> 130 us  [fused(): pl.pallas_call(functools.partial(kernel, line, n_tp, native, parts), out_...]
    convert_element_type x1 -> x0, local copies, waits for them, and re-layouts: 1.87 us -> none  [per_device(): d_w_up = d_w.transpose(1, 0, 2).reshape(rows, block).astype(F32)]
    convert_element_type x1, other arithmetic: 1.5 us -> 2.91 us  [per_device(): return (d_in.reshape(inputs.shape), d_w.astype(F32))]
where the time goes in v1:
time: 135 us
  Pallas kernels  130 us (96%)
  other arithmetic  2.91 us (2%)
    pallas_call x1, Pallas kernels, fused(): pl.pallas_call(functools.partial(kernel, line, n_tp, native, parts), out_...  130 us
    convert_element_type x1, other arithmetic, per_device(): return (d_in.reshape(inputs.shape), d_w.astype(F32))  2.91 us

profile of v1, /device:TPU:0, one launch (start us, length us, event | category | flops | bytes accessed | tf_op | source)
XLA Modules:
  0.0 134.6 jit_solution(9562126705641194980)
XLA Ops:
  0.6 129.9 %fused.1 = (bf16[256,2048]{1,0:T(8,128)(2,1)}, bf16[2,192,2048]{2,1,0:T(8,128)(2,1)}) custom-call(bf16[384,2048]{1,0:T(8,128)(2,1)} %x_in.1, bf16[384,2048]{1,0:T(8,128)(2,1)} %c_in.1, bf16[256,2048]{1,0:T(8,128)(2,1)} %up_in.1, bf16[2048,256]{1,0:T(8,128)(2,1)} %down_in.1), custom_call_target="tpu_custom_call" | custom-call | tf_op jit(solution)/shard_map/fused/pallas_call | solution.py:527
  130.6 0.0 copy-start
  130.6 2.9 %convert_element_type.3 = f32[256,2048]{1,0:T(8,128)} convert(bf16[256,2048]{1,0:T(8,128)(2,1)} %get-tuple-element.5) | non-fusion elementwise | flops 524288 | bytes 3145728 | tf_op jit(solution)/shard_map/convert_element_type | solution.py:566
  133.5 0.0 copy-done
  133.5 1.1 copy.7
Async XLA Ops:
  130.6 2.9 %copy-start = (bf16[2,192,2048]{2,1,0:T(8,128)(2,1)S(1)}, bf16[2,192,2048]{2,1,0:T(8,128)(2,1)}, u32[]{:S(2)}) copy-start(bf16[2,192,2048]{2,1,0:T(8,128)(2,1)} %get-tuple-element.4) | copy-start | bytes 4718596

commit v2 on v1

--- a/solution.py
+++ b/solution.py
@@ -135,9 +135,13 @@
     first[2, 1].start()
     first[1, 1].start()
     first[2, 0].start()
+    most = half // 48 * 32
+    base = pl.multiple_of(core * half, half)
+    lead, rest = pl.ds(base, most), pl.ds(base + most, half - most)
     diag = [
-        remote(xs.at[0, 1, mine], xs.at[0, 3, mine], ts.at[2, 0], tr.at[2, 0], to_y),
+        remote(xs.at[0, 1, lead], xs.at[0, 3, lead], ts.at[2, 0], tr.at[2, 0], to_y),
         remote(xs.at[1, 2, mine], xs.at[1, 3, mine], ts.at[2, 1], tr.at[2, 1], to_x),
+        remote(xs.at[0, 2, rest], xs.at[0, 3, rest], ts.at[3, 0], tr.at[3, 0], to_x),
     ]
 
     def swap(slot, a):
@@ -247,8 +251,12 @@
                     diag[0].start()
                 if (slot, a) == (2, 1):
                     diag[1].start()
+                if (slot, a) == (2, 0):
+                    diag[2].start()
             else:
                 diag[a].wait_recv()
+                if a == 0:
+                    diag[2].wait_recv()
             swap(slot, a).start()
         return run
 
@@ -279,8 +287,8 @@
             (1, 2, 0): [use(2, 0)],
             (1, 2, 1): [got(3, 1)],
             (1, 2, 2): [use(3, 1)],
-            (1, 3, 1): [got(3, 0)],
-            (1, 3, 2): [use(3, 0), early],
+            (1, 2, 3): [got(3, 0)],
+            (1, 3, 0): [use(3, 0), early],
         }
         steps = [(0, 1)]
         for s in range(2, line):
@@ -345,7 +353,7 @@
             total = total + tpin[k - 1, slot].astype(F32)
         return total
 
-    cut = (width * 3 // 8) // 128 * 128
+    cut = width * 7 // 16 // 128 * 128
     left, right = pl.ds(0, cut), pl.ds(cut, width - cut)
     q_copies = {
         "x3": remote(part_.at[3, c, :, left], q1.at[1, :, left], qs.at[0], qr.at[0], to_x),
@@ -409,13 +417,13 @@
         remote(blk, blk, es.at[1, h], er.at[1, h], to_y).wait_recv()
         e_r[h].start()
 
-    def in_first():
+    def in_x3():
         q_copies["x3"].wait_recv()
         part_[2, c, :, left] = (part_[2, c, :, left].astype(F32) + q1[1, :, left].astype(F32)).astype(BF16)
-        q_copies["y2r"].start()
+
+    def in_y3():
         q_copies["y3"].wait_recv()
         part_[1, c, :, right] = (part_[1, c, :, right].astype(F32) + q1[1, :, right].astype(F32)).astype(BF16)
-        q_copies["x1r"].start()
 
     out_own = pltpu.make_async_copy(fo, din_out.at[c], dl.at[0])
     out_peers = [
@@ -435,38 +443,51 @@
         if line > 1:
             grow_slot(1, final, line - 1, slot)
         make_g(final, slot)
-        make_part(slot)
+
+    def send(*names):
+        for name in names:
+            q_copies[name].start()
+
+    def sums(h, lo, hi):
+        for t in range(lo, min(hi, line)):
+            o_step(h, t)
+
+    def weights(lo, hi):
+        for i in range(lo, min(hi, line)):
+            make_dw(final, i)
 
     last_rows(3)
-    last_rows(1)
+    make_part(3)
+    for slot in (1, 2, 0):
+        last_rows(slot)
+    make_part(1)
     store_sum(3)
-    q_copies["x3"].start()
-    q_copies["y3"].start()
+    send("x3", "y3")
     if parts > 1:
-        o_step(0, 1)
-    last_rows(2)
+        sums(0, 1, 2)
+    weights(0, 1)
+    make_part(2)
     store_sum(1)
-    q_copies["x1"].start()
+    send("x1")
+    weights(1, 2)
     store_sum(2)
-    q_copies["y2"].start()
-    last_rows(0)
-    for i in range(line):
-        make_dw(final, i)
-    if parts == 1 and line > 1:
-        o_step(0, 1)
-    for t in range(2, line - 1):
-        o_step(0, t)
-    in_first()
+    send("y2")
+    make_part(0)
+    weights(2, line)
+    if parts == 1:
+        sums(0, 1, 2)
+    sums(0, 2, line - 1)
+    in_x3()
     if line > 2:
-        o_step(0, line - 1)
+        sums(0, line - 1, line)
     finish(0)
+    send("y2r")
+    in_y3()
+    send("x1r")
     for h in range(1, parts):
-        for t in range(1, line):
-            o_step(h, t)
-            if t == 1:
-                relay(h - 1)
-        if line == 1:
-            relay(h - 1)
+        sums(h, 1, line - 1)
+        relay(h - 1)
+        sums(h, max(line - 1, 1), line)
         finish(h)
     in_last()
     relay(final)
@@ -547,7 +568,7 @@
             vmem(part, width),
             vmem(part, width),
             dma((2, parts, line, 4)), dma((2, parts, line, 4)), dma((parts, 2)), dma((parts, 2)),
-            dma((3, 2)), dma((3, 2)), dma((3, 2)), dma((3, 2)), dma((2 + 2 * parts,)),
+            dma((4, 2)), dma((4, 2)), dma((3, 2)), dma((3, 2)), dma((2 + 2 * parts,)),
             dma((2, parts, line)), dma((2, parts, line)),
             dma((3, parts)), dma((3, parts)), dma((parts,)),
             dma((others, 4)), dma((others, 4)), dma((6,)), dma((6,)),

time: 135 us -> 125 us (0.926)
  Pallas kernels: 130 us -> 121 us
    pallas_call x1, Pallas kernels: 130 us -> 121 us  [fused(): pl.pallas_call(functools.partial(kernel, line, n_tp, native, parts), out_...]
where the time goes in v2:
time: 125 us
  Pallas kernels  121 us (97%)
  other arithmetic  2.91 us (2%)
    pallas_call x1, Pallas kernels, fused(): pl.pallas_call(functools.partial(kernel, line, n_tp, native, parts), out_...  121 us
    convert_element_type x1, other arithmetic, per_device(): return (d_in.reshape(inputs.shape), d_w.astype(F32))  2.91 us

profile of v2, /device:TPU:0, one launch (start us, length us, event | category | flops | bytes accessed | tf_op | source)
XLA Modules:
  0.0 125.3 jit_solution(10543052349197758829)
XLA Ops:
  0.6 120.6 %fused.1 = (bf16[256,2048]{1,0:T(8,128)(2,1)}, bf16[2,192,2048]{2,1,0:T(8,128)(2,1)}) custom-call(bf16[384,2048]{1,0:T(8,128)(2,1)} %x_in.1, bf16[384,2048]{1,0:T(8,128)(2,1)} %c_in.1, bf16[256,2048]{1,0:T(8,128)(2,1)} %up_in.1, bf16[2048,256]{1,0:T(8,128)(2,1)} %down_in.1), custom_call_target="tpu_custom_call" | custom-call | tf_op jit(solution)/shard_map/fused/pallas_call | solution.py:548
  121.3 0.0 copy-start
  121.3 2.9 %convert_element_type.3 = f32[256,2048]{1,0:T(8,128)} convert(bf16[256,2048]{1,0:T(8,128)(2,1)} %get-tuple-element.5) | non-fusion elementwise | flops 524288 | bytes 3145728 | tf_op jit(solution)/shard_map/convert_element_type | solution.py:587
  124.2 0.0 copy-done
  124.2 1.1 copy.7
Async XLA Ops:
  121.3 2.9 %copy-start = (bf16[2,192,2048]{2,1,0:T(8,128)(2,1)S(1)}, bf16[2,192,2048]{2,1,0:T(8,128)(2,1)}, u32[]{:S(2)}) copy-start(bf16[2,192,2048]{2,1,0:T(8,128)(2,1)} %get-tuple-element.4) | copy-start | bytes 4718596

commit v3 on v2

--- a/solution.py
+++ b/solution.py
@@ -194,9 +194,8 @@
 
         lax.fori_loop(0, 2 * n, body, 0)
 
-    def join(slot, u):
-        ready[u] += 1
-        for h in range(parts):
+    def join(slot, u, halves):
+        for h in halves:
             lo, hi = jnp.maximum(at - done[h][u], 0), jnp.minimum(at + done[h][u], line - 1)
 
             def body(lvl, _):
@@ -210,9 +209,13 @@
 
     low = at < line - at - 1
 
-    def o_copy(go_up, h, o):
-        d = 0 if go_up else 1
-        return remote(dw.at[h, o], zin.at[d, h, o], os.at[d, h, o], orr.at[d, h, o], up if go_up else down)
+    turns = (1 - p, p)
+
+    def o_copy(go_up, h, o, k):
+        d, b = 0 if go_up else 1, turns[k]
+        return remote(
+            dw.at[h, o, b], zin.at[d, h, o, b], os.at[d, h, o, k], orr.at[d, h, o, k], up if go_up else down
+        )
 
     def make_dw(h, i):
         o = jnp.where(low, line - 1 - i, i)
@@ -223,11 +226,13 @@
         if i < line - 1:
             @pl.when(at == 0)
             def _():
-                o_copy(True, h, line - 1 - i).start()
+                for k in (0, 1):
+                    o_copy(True, h, line - 1 - i, k).start()
 
             @pl.when(at == line - 1)
             def _():
-                o_copy(False, h, i).start()
+                for k in (0, 1):
+                    o_copy(False, h, i, k).start()
 
     own_x.wait()
     own_c.wait()
@@ -263,11 +268,16 @@
     def use(slot, a):
         def run():
             swapped(slot, a)
-            join(slot, a)
+            ready[a] += 1
+            join(slot, a, range(parts))
         return run
 
     def early():
+        swapped(3, 0)
+        ready[0] += 1
         for h in range(final):
+            join(3, 0, [h])
+
             def body(slot, _):
                 make_g(h, slot)
                 return 0
@@ -275,6 +285,7 @@
             lax.fori_loop(0, 4, body, 0)
             for i in range(line):
                 make_dw(h, i)
+        join(3, 0, [final])
 
     if parts == 2:
         hooks = {
@@ -286,9 +297,8 @@
             (0, 3, 3): [got(2, 0)],
             (1, 2, 0): [use(2, 0)],
             (1, 2, 1): [got(3, 1)],
-            (1, 2, 2): [use(3, 1)],
-            (1, 2, 3): [got(3, 0)],
-            (1, 3, 0): [use(3, 0), early],
+            (1, 2, 2): [use(3, 1), got(3, 0)],
+            (1, 2, 3): [early],
         }
         steps = [(0, 1)]
         for s in range(2, line):
@@ -305,7 +315,7 @@
             (0, 3, 0): [use(2, 0), got(3, 1)],
             (0, 3, 1): [use(3, 1)],
             (0, 3, 2): [got(3, 0)],
-            (0, 3, 3): [use(3, 0), early],
+            (0, 3, 3): [early],
         }
         steps = [(0, s) for s in range(1, line)]
     for h, s in steps:
@@ -345,6 +355,23 @@
         for k in range(1, n_tp):
             p_copy(slot, k).start()
 
+    def make_part_rows(slot):
+        for k in list(range(1, n_tp)) + [0]:
+            there = lax.rem(c + k, n_tp)
+            tok = pl.ds(pl.multiple_of(there * part, part), part)
+
+            def body(lvl, _):
+                span = pl.ds(pl.multiple_of(lvl * level, level), level)
+                value = dot(g[0, slot, tok], wu[0, lvl].reshape(level, cols), 1, 1)
+                for h in range(1, parts):
+                    value = value + dot(g[h, slot, tok], wu[h, lvl].reshape(level, cols), 1, 1)
+                part_[slot, there, :, span] = value.astype(BF16)
+                return 0
+
+            lax.fori_loop(0, line, body, 0)
+            if k > 0:
+                p_copy(slot, k).start()
+
     def tp_sum(slot):
         for k in range(1, n_tp):
             p_copy(slot, k).wait_recv()
@@ -367,10 +394,8 @@
     def store_sum(slot):
         part_[slot, c] = tp_sum(slot).astype(BF16)
 
-    def add_in(d, h, o):
-        dw[h, o] = (dw[h, o].astype(F32) + zin[d, h, o].astype(F32)).astype(BF16)
-
-    def o_step(h, t):
+    def o_step(h, t, k):
+        b = turns[k]
         for go_up in (True, False):
             d = 0 if go_up else 1
             gap = at if go_up else line - 1 - at
@@ -378,44 +403,56 @@
 
             @pl.when((gap > 0) & (gap <= t))
             def _():
-                o_copy(go_up, h, o).wait_recv()
+                o_copy(go_up, h, o, k).wait_recv()
                 if t < line - 1:
-                    add_in(d, h, o)
-                    o_copy(go_up, h, o).start()
-
-    def dw_at(q, h):
-        return dw_out.at[:, pl.ds(pl.multiple_of((q * parts + h) * cols, cols), cols)]
-
-    e_x, e_y, e_own, e_r = [], [], [], []
-    for h in range(parts):
-        here, across = dw_at(quarter, h), dw_at(2 * r + 1 - p, h)
-        e_x.append(remote(fin.at[h, p], here, es.at[0, h], er.at[0, h], to_x))
-        e_y.append(remote(fin.at[h, 1 - p], here, es.at[1, h], er.at[1, h], to_y))
-        e_own.append(pltpu.make_async_copy(fin.at[h, p], here, el.at[h]))
-        e_r.append(remote(across, across, es.at[2, h], er.at[2, h], to_x))
-
-    def finish(h):
-        if line == 1:
-            fin[h] = dw[h, at]
+                    dw[h, o, b] = (dw[h, o, b].astype(F32) + zin[d, h, o, b].astype(F32)).astype(BF16)
+                    o_copy(go_up, h, o, k).start()
+
+    half_rows = [pl.ds(i * (rows // 2), rows // 2) for i in (0, 1)]
+
+    def dw_at(q, h, span=slice(None)):
+        return dw_out.at[span, pl.ds(pl.multiple_of((q * parts + h) * cols, cols), cols)]
+
+    def e_y(h, i):
+        here = dw_at(quarter, h, half_rows[i])
+        return remote(fin.at[h, 1 - p, half_rows[i]], here, es.at[1, h, i], er.at[1, h, i], to_y)
+
+    def e_relay(h, i):
+        here = dw_at(2 * r + 1 - p, h, half_rows[i])
+        return remote(here, here, es.at[2, h, i], er.at[2, h, i], to_x)
+
+    def e_x(h):
+        return remote(fin.at[h, p], dw_at(quarter, h), es.at[0, h, 0], er.at[0, h, 0], to_x)
+
+    def e_own(h):
+        return pltpu.make_async_copy(fin.at[h, p], dw_at(quarter, h), el.at[h])
+
+    def finish(h, k):
+        b = turns[k]
         for d, there in ((0, has_down), (1, has_up)):
-            if line > 1:
-                @pl.when(there & jnp.logical_not(has_up & has_down))
-                def _():
-                    fin[h] = (dw[h, at].astype(F32) + zin[d, h, at].astype(F32)).astype(BF16)
+            @pl.when(there & jnp.logical_not(has_up & has_down))
+            def _():
+                fin[h, b] = (dw[h, at, b].astype(F32) + zin[d, h, at, b].astype(F32)).astype(BF16)
 
         @pl.when(has_up & has_down)
         def _():
-            total = dw[h, at].astype(F32) + zin[0, h, at].astype(F32) + zin[1, h, at].astype(F32)
-            fin[h] = total.astype(BF16)
-
-        e_x[h].start()
-        e_y[h].start()
-        e_own[h].start()
+            total = dw[h, at, b].astype(F32) + zin[0, h, at, b].astype(F32) + zin[1, h, at, b].astype(F32)
+            fin[h, b] = total.astype(BF16)
+
+        if line == 1:
+            fin[h, b] = dw[h, at, b]
+        if k == 0:
+            e_y(h, 0).start()
+            e_y(h, 1).start()
+        else:
+            e_x(h).start()
+            e_own(h).start()
 
     def relay(h):
-        blk = dw_at(2 * r + 1 - p, h)
-        remote(blk, blk, es.at[1, h], er.at[1, h], to_y).wait_recv()
-        e_r[h].start()
+        for i in (0, 1):
+            blk = dw_at(2 * r + 1 - p, h, half_rows[i])
+            remote(blk, blk, es.at[1, h, i], er.at[1, h, i], to_y).wait_recv()
+            e_relay(h, i).start()
 
     def in_x3():
         q_copies["x3"].wait_recv()
@@ -448,61 +485,78 @@
         for name in names:
             q_copies[name].start()
 
-    def sums(h, lo, hi):
-        for t in range(lo, min(hi, line)):
-            o_step(h, t)
+    def sums(h, t, k):
+        if 1 <= t < line:
+            o_step(h, t, k)
 
     def weights(lo, hi):
         for i in range(lo, min(hi, line)):
             make_dw(final, i)
 
+    def close(h):
+        for k in (0, 1):
+            sums(h, line - 1, k)
+            finish(h, k)
+
+    split = parts > 1
     last_rows(3)
-    make_part(3)
+    make_part_rows(3)
     for slot in (1, 2, 0):
         last_rows(slot)
-    make_part(1)
     store_sum(3)
     send("x3", "y3")
-    if parts > 1:
-        sums(0, 1, 2)
+    if split:
+        sums(0, 1, 0)
+    make_part(1)
+    if split:
+        sums(0, 1, 1)
     weights(0, 1)
     make_part(2)
     store_sum(1)
     send("x1")
+    if split:
+        sums(0, 2, 0)
     weights(1, 2)
+    make_part(0)
     store_sum(2)
     send("y2")
-    make_part(0)
+    if split:
+        sums(0, 2, 1)
     weights(2, line)
-    if parts == 1:
-        sums(0, 1, 2)
-    sums(0, 2, line - 1)
+    for t in range(3 if split else 1, line - 1):
+        for k in (0, 1):
+            sums(0, t, k)
+    close(0)
     in_x3()
-    if line > 2:
-        sums(0, line - 1, line)
-    finish(0)
     send("y2r")
     in_y3()
     send("x1r")
     for h in range(1, parts):
-        sums(h, 1, line - 1)
+        for t in range(1, line - 1):
+            for k in (0, 1):
+                sums(h, t, k)
         relay(h - 1)
-        sums(h, max(line - 1, 1), line)
-        finish(h)
+        close(h)
     in_last()
     relay(final)
 
     for k in range(1, n_tp):
         out_peers[k - 1].wait_recv()
     for h in range(parts):
-        for q, col in ((2 * (1 - r) + p, 0), (2 * (1 - r) + 1 - p, 2)):
-            blk = dw_at(q, h)
-            remote(blk, blk, es.at[col, h], er.at[col, h], to_x).wait_recv()
+        blk = dw_at(2 * (1 - r) + p, h)
+        remote(blk, blk, es.at[0, h, 0], er.at[0, h, 0], to_x).wait_recv()
+        for i in (0, 1):
+            blk = dw_at(2 * (1 - r) + 1 - p, h, half_rows[i])
+            remote(blk, blk, es.at[2, h, i], er.at[2, h, i], to_x).wait_recv()
     out_own.wait()
-    for copy in e_own:
-        copy.wait()
-    for copy in out_peers + e_x + e_y + e_r + list(q_copies.values()):
+    for copy in out_peers + list(q_copies.values()):
         copy.wait_send()
+    for h in range(parts):
+        e_own(h).wait()
+        e_x(h).wait_send()
+        for i in (0, 1):
+            e_y(h, i).wait_send()
+            e_relay(h, i).wait_send()
     for slot in range(4):
         for k in range(1, n_tp):
             p_copy(slot, k).wait_send()
@@ -510,11 +564,13 @@
         for o in range(line):
             @pl.when((at < o) & has_up)
             def _():
-                o_copy(True, h, o).wait_send()
+                for k in (0, 1):
+                    o_copy(True, h, o, k).wait_send()
 
             @pl.when((at > o) & has_down)
             def _():
-                o_copy(False, h, o).wait_send()
+                for k in (0, 1):
+                    o_copy(False, h, o, k).wait_send()
     for slot in (1, 2, 3):
         for a in (0, 1):
             swap(slot, a).wait_send()
@@ -569,8 +625,8 @@
             vmem(part, width),
             dma((2, parts, line, 4)), dma((2, parts, line, 4)), dma((parts, 2)), dma((parts, 2)),
             dma((4, 2)), dma((4, 2)), dma((3, 2)), dma((3, 2)), dma((2 + 2 * parts,)),
-            dma((2, parts, line)), dma((2, parts, line)),
-            dma((3, parts)), dma((3, parts)), dma((parts,)),
+            dma((2, parts, line, 2)), dma((2, parts, line, 2)),
+            dma((4, parts, 2)), dma((4, parts, 2)), dma((parts,)),
             dma((others, 4)), dma((others, 4)), dma((6,)), dma((6,)),
             dma((others,)), dma((others,)), dma((1,)),
         ],

time: 125 us -> 123 us (0.984)
  Pallas kernels: 121 us -> 118 us
    pallas_call x1, Pallas kernels: 121 us -> 118 us  [fused(): pl.pallas_call(functools.partial(kernel, line, n_tp, native, parts), out_...]
where the time goes in v3:
time: 123 us
  Pallas kernels  118 us (96%)
  other arithmetic  2.91 us (2%)
    pallas_call x1, Pallas kernels, fused(): pl.pallas_call(functools.partial(kernel, line, n_tp, native, parts), out_...  118 us
    convert_element_type x1, other arithmetic, per_device(): return (d_in.reshape(inputs.shape), d_w.astype(F32))  2.91 us

profile of v3, /device:TPU:0, one launch (start us, length us, event | category | flops | bytes accessed | tf_op | source)
XLA Modules:
  0.0 122.9 jit_solution(8015364877151387232)
XLA Ops:
  0.6 118.2 %fused.1 = (bf16[256,2048]{1,0:T(8,128)(2,1)}, bf16[2,192,2048]{2,1,0:T(8,128)(2,1)}) custom-call(bf16[384,2048]{1,0:T(8,128)(2,1)} %x_in.1, bf16[384,2048]{1,0:T(8,128)(2,1)} %c_in.1, bf16[256,2048]{1,0:T(8,128)(2,1)} %up_in.1, bf16[2048,256]{1,0:T(8,128)(2,1)} %down_in.1), custom_call_target="tpu_custom_call" | custom-call | tf_op jit(solution)/shard_map/fused/pallas_call | solution.py:604
  118.8 0.0 copy-start
  118.8 2.9 %convert_element_type.3 = f32[256,2048]{1,0:T(8,128)} convert(bf16[256,2048]{1,0:T(8,128)(2,1)} %get-tuple-element.5) | non-fusion elementwise | flops 524288 | bytes 3145728 | tf_op jit(solution)/shard_map/convert_element_type | solution.py:643
  121.7 0.0 copy-done
  121.7 1.1 copy.7
Async XLA Ops:
  118.8 2.9 %copy-start = (bf16[2,192,2048]{2,1,0:T(8,128)(2,1)S(1)}, bf16[2,192,2048]{2,1,0:T(8,128)(2,1)}, u32[]{:S(2)}) copy-start(bf16[2,192,2048]{2,1,0:T(8,128)(2,1)} %get-tuple-element.4) | copy-start | bytes 4718596

commit v4 on v3

--- a/solution.py
+++ b/solution.py
@@ -16,7 +16,7 @@
 
 
 def kernel(line, n_tp, native, parts, x_in, c_in, up_in, down_in, dw_out, din_out,
-           xs, wu, wd, acc, g, dw, zin, fin, part_, tpin, q1, q2, fo,
+           xs, wu, wd, acc, g, dw, zin, fin, part_, tpin, q1, q2, fo, ahead,
            zs, zr, ys, yr, ts, tr, cs, cr, ls, os, orr, es, er, el, ps, pr, qs, qr, ds, dr, dl):
     r, f, c = lax.axis_index("rep"), lax.axis_index("fs"), lax.axis_index("tp")
     p, at = lax.rem(f, 2), lax.div(f, 2)
@@ -234,6 +234,17 @@
                 for k in (0, 1):
                     o_copy(False, h, i, k).start()
 
+    part = tokens // n_tp
+
+    def start_part(slot):
+        def body(lvl, _):
+            span = pl.ds(pl.multiple_of(lvl * level, level), level)
+            value = dot(g[0, slot], wu[0, lvl].reshape(level, cols), 1, 1)
+            ahead[:, :, span] = value.reshape(n_tp, part, level)
+            return 0
+
+        lax.fori_loop(0, line, body, 0)
+
     own_x.wait()
     own_c.wait()
     for copy in own_w:
@@ -286,6 +297,8 @@
             for i in range(line):
                 make_dw(h, i)
         join(3, 0, [final])
+        if parts > 1:
+            start_part(3)
 
     if parts == 2:
         hooks = {
@@ -340,8 +353,6 @@
             part_.at[slot, there], tpin.at[k - 1, slot], ps.at[k - 1, slot], pr.at[k - 1, slot], {"tp": there}
         )
 
-    part = tokens // n_tp
-
     def make_part(slot):
         def body(lvl, _):
             span = pl.ds(pl.multiple_of(lvl * level, level), level)
@@ -355,16 +366,14 @@
         for k in range(1, n_tp):
             p_copy(slot, k).start()
 
-    def make_part_rows(slot):
+    def end_part(slot):
         for k in list(range(1, n_tp)) + [0]:
             there = lax.rem(c + k, n_tp)
             tok = pl.ds(pl.multiple_of(there * part, part), part)
 
             def body(lvl, _):
                 span = pl.ds(pl.multiple_of(lvl * level, level), level)
-                value = dot(g[0, slot, tok], wu[0, lvl].reshape(level, cols), 1, 1)
-                for h in range(1, parts):
-                    value = value + dot(g[h, slot, tok], wu[h, lvl].reshape(level, cols), 1, 1)
+                value = ahead[there, :, span] + dot(g[1, slot, tok], wu[1, lvl].reshape(level, cols), 1, 1)
                 part_[slot, there, :, span] = value.astype(BF16)
                 return 0
 
@@ -380,14 +389,17 @@
             total = total + tpin[k - 1, slot].astype(F32)
         return total
 
-    cut = width * 7 // 16 // 128 * 128
+    cut = width * 3 // 8 // 128 * 128
+    early_cut = cut // 256 * 128
     left, right = pl.ds(0, cut), pl.ds(cut, width - cut)
+    left_a, left_b = pl.ds(0, early_cut), pl.ds(early_cut, cut - early_cut)
     q_copies = {
         "x3": remote(part_.at[3, c, :, left], q1.at[1, :, left], qs.at[0], qr.at[0], to_x),
         "y3": remote(part_.at[3, c, :, right], q1.at[1, :, right], qs.at[1], qr.at[1], to_y),
         "x1": remote(part_.at[1, c, :, left], q1.at[0, :, left], qs.at[2], qr.at[2], to_x),
         "y2": remote(part_.at[2, c, :, right], q1.at[0, :, right], qs.at[3], qr.at[3], to_y),
-        "y2r": remote(part_.at[2, c, :, left], q2.at[:, left], qs.at[4], qr.at[4], to_y),
+        "y2a": remote(part_.at[2, c, :, left_a], q2.at[:, left_a], qs.at[4], qr.at[4], to_y),
+        "y2b": remote(part_.at[2, c, :, left_b], q2.at[:, left_b], qs.at[6], qr.at[6], to_y),
         "x1r": remote(part_.at[1, c, :, right], q2.at[:, right], qs.at[5], qr.at[5], to_x),
     }
 
@@ -462,19 +474,29 @@
         q_copies["y3"].wait_recv()
         part_[1, c, :, right] = (part_[1, c, :, right].astype(F32) + q1[1, :, right].astype(F32)).astype(BF16)
 
-    out_own = pltpu.make_async_copy(fo, din_out.at[c], dl.at[0])
-    out_peers = [
-        remote(fo, din_out.at[c], ds.at[k - 1], dr.at[k - 1], {"tp": lax.rem(c + k, n_tp)}) for k in range(1, n_tp)
-    ]
-
-    def in_last():
-        total = tp_sum(0)
-        for name in ("x1", "y2", "y2r", "x1r"):
+    segments = ((right, ("y2", "x1r")), (left_a, ("x1", "y2a")), (left_b, ("y2b",)))
+
+    def out_own(i):
+        span = segments[i][0]
+        return pltpu.make_async_copy(fo.at[:, span], din_out.at[c, :, span], dl.at[i])
+
+    def out_peer(i, k):
+        span = segments[i][0]
+        return remote(
+            fo.at[:, span], din_out.at[c, :, span], ds.at[k - 1, i], dr.at[k - 1, i], {"tp": lax.rem(c + k, n_tp)}
+        )
+
+    def in_last(i):
+        span, names = segments[i]
+        for name in names:
             q_copies[name].wait_recv()
-        fo[...] = (total + q1[0].astype(F32) + q2[...].astype(F32)).astype(BF16)
-        out_own.start()
-        for copy in out_peers:
-            copy.start()
+        total = part_[0, c, :, span].astype(F32)
+        for k in range(1, n_tp):
+            total = total + tpin[k - 1, 0, :, span].astype(F32)
+        fo[:, span] = (total + q1[0, :, span].astype(F32) + q2[:, span].astype(F32)).astype(BF16)
+        out_own(i).start()
+        for k in range(1, n_tp):
+            out_peer(i, k).start()
 
     def last_rows(slot):
         if line > 1:
@@ -497,10 +519,15 @@
         for k in (0, 1):
             sums(h, line - 1, k)
             finish(h, k)
+            if (h, k) == (final, 0):
+                send("y2b")
 
     split = parts > 1
     last_rows(3)
-    make_part_rows(3)
+    if split:
+        end_part(3)
+    else:
+        make_part(3)
     for slot in (1, 2, 0):
         last_rows(slot)
     store_sum(3)
@@ -526,30 +553,39 @@
     for t in range(3 if split else 1, line - 1):
         for k in (0, 1):
             sums(0, t, k)
-    close(0)
+    if split:
+        close(0)
     in_x3()
-    send("y2r")
+    send("y2a")
     in_y3()
     send("x1r")
+    if not split:
+        close(0)
     for h in range(1, parts):
         for t in range(1, line - 1):
             for k in (0, 1):
                 sums(h, t, k)
         relay(h - 1)
         close(h)
-    in_last()
+    for k in range(1, n_tp):
+        p_copy(0, k).wait_recv()
+    in_last(0)
+    in_last(1)
     relay(final)
-
-    for k in range(1, n_tp):
-        out_peers[k - 1].wait_recv()
+    in_last(2)
+
+    for i in range(3):
+        out_own(i).wait()
+        for k in range(1, n_tp):
+            out_peer(i, k).wait_recv()
+            out_peer(i, k).wait_send()
     for h in range(parts):
         blk = dw_at(2 * (1 - r) + p, h)
         remote(blk, blk, es.at[0, h, 0], er.at[0, h, 0], to_x).wait_recv()
         for i in (0, 1):
             blk = dw_at(2 * (1 - r) + 1 - p, h, half_rows[i])
             remote(blk, blk, es.at[2, h, i], er.at[2, h, i], to_x).wait_recv()
-    out_own.wait()
-    for copy in out_peers + list(q_copies.values()):
+    for copy in q_copies.values():
         copy.wait_send()
     for h in range(parts):
         e_own(h).wait()
@@ -623,15 +659,16 @@
             vmem(2, part, width),
             vmem(part, width),
             vmem(part, width),
+            pltpu.VMEM((n_tp, part, width) if parts > 1 else (1, 8, 128), F32),
             dma((2, parts, line, 4)), dma((2, parts, line, 4)), dma((parts, 2)), dma((parts, 2)),
             dma((4, 2)), dma((4, 2)), dma((3, 2)), dma((3, 2)), dma((2 + 2 * parts,)),
             dma((2, parts, line, 2)), dma((2, parts, line, 2)),
             dma((4, parts, 2)), dma((4, parts, 2)), dma((parts,)),
-            dma((others, 4)), dma((others, 4)), dma((6,)), dma((6,)),
-            dma((others,)), dma((others,)), dma((1,)),
+            dma((others, 4)), dma((others, 4)), dma((7,)), dma((7,)),
+            dma((others, 3)), dma((others, 3)), dma((3,)),
         ],
         compiler_params=pltpu.CompilerParams(
-            collective_id=0, has_side_effects=True, vmem_limit_bytes=60 * 2**20
+            collective_id=0, has_side_effects=True, vmem_limit_bytes=52 * 2**20
         ),
         name="fused",
     )(x, c, w_up, w_down)

time: 123 us -> 120 us (0.976)
  other arithmetic: 2.91 us -> 1.57 us
    pallas_call x1, Pallas kernels: 118 us -> 117 us  [fused(): pl.pallas_call(functools.partial(kernel, line, n_tp, native, parts), out_...]
    convert_element_type x1, other arithmetic: 2.91 us -> 1.57 us  [per_device(): return (d_in.reshape(inputs.shape), d_w.astype(F32))]
where the time goes in v4:
time: 120 us
  Pallas kernels  117 us (98%)
  other arithmetic  1.57 us (1%)
  local copies, waits for them, and re-layouts  1.47 us (1%)
    pallas_call x1, Pallas kernels, fused(): pl.pallas_call(functools.partial(kernel, line, n_tp, native, parts), out_...  117 us

profile of v4, /device:TPU:0, one launch (start us, length us, event | category | flops | bytes accessed | tf_op | source)
XLA Modules:
  0.0 120.2 jit_solution(10816814246679128860)
XLA Ops:
  0.6 116.5 %fused.1 = (bf16[256,2048]{1,0:T(8,128)(2,1)S(1)}, bf16[2,192,2048]{2,1,0:T(8,128)(2,1)}) custom-call(bf16[384,2048]{1,0:T(8,128)(2,1)} %x_in.1, bf16[384,2048]{1,0:T(8,128)(2,1)} %c_in.1, bf16[256,2048]{1,0:T(8,128)(2,1)} %up_in.1, bf16[2048,256]{1,0:T(8,128)(2,1)} %down_in.1), custom_call_target="tpu_custom_call" | custom-call | tf_op jit(solution)/shard_map/fused/pallas_call | solution.py:640
  117.2 0.0 copy-start
  117.2 1.6 %convert_element_type.3 = f32[256,2048]{1,0:T(8,128)} convert(bf16[256,2048]{1,0:T(8,128)(2,1)S(1)} %get-tuple-element.5) | non-fusion elementwise | flops 524288 | bytes 3145728 | tf_op jit(solution)/shard_map/convert_element_type | solution.py:680
  118.7 0.3 copy-done
  119.1 1.1 copy.7
Async XLA Ops:
  117.2 1.9 %copy-start = (bf16[2,192,2048]{2,1,0:T(8,128)(2,1)S(1)}, bf16[2,192,2048]{2,1,0:T(8,128)(2,1)}, u32[]{:S(2)}) copy-start(bf16[2,192,2048]{2,1,0:T(8,128)(2,1)} %get-tuple-element.4) | copy-start | bytes 4718596

commit v5 on v4

--- a/solution.py
+++ b/solution.py
@@ -61,9 +61,9 @@
         return (up_in, down_in)[u].at[:, span]
 
     own_x = pltpu.make_async_copy(x_in, xs.at[0, 0], ls.at[0])
-    own_c = pltpu.make_async_copy(c_in, xs.at[1, 0], ls.at[1])
+    own_c = pltpu.make_async_copy(c_in, xs.at[1, 0], ls.at[0])
     own_w = [
-        pltpu.make_async_copy(own_block(u, quarter, h), ws[u].at[h, at, p], ls.at[2 + 2 * h + u])
+        pltpu.make_async_copy(own_block(u, quarter, h), ws[u].at[h, at, p], ls.at[1])
         for h in range(parts) for u in (0, 1)
     ]
     own_x.start()
@@ -84,13 +84,13 @@
         pl.semaphore_wait(barrier, n_near + 1 if line > 1 else n_near)
 
     y_copies = [
-        remote(own_block(u, 2 * r + 1 - p, h), ws[u].at[h, at, p], ys.at[h, u], yr.at[h, u], to_y)
+        remote(own_block(u, 2 * r + 1 - p, h), ws[u].at[h, at, p], ys.at[0], yr.at[h, u], to_y)
         for h in range(parts) for u in (0, 1)
     ]
 
     def y_arrival(u, h):
         blk = ws[u].at[h, at, 1 - p]
-        return remote(blk, blk, ys.at[h, u], yr.at[h, u], to_y)
+        return remote(blk, blk, ys.at[0], yr.at[h, u], to_y)
 
     for copy in y_copies:
         copy.start()
@@ -101,7 +101,7 @@
         blk = ws[u].at[h, lvl, p if own_pair else 1 - p]
         src = own_block(u, quarter, h) if (s == 0 and own_pair) else blk
         d = 0 if go_up else 1
-        return remote(src, blk, zs.at[d, h, s, j], zr.at[d, h, s, j], up if go_up else down)
+        return remote(src, blk, zs.at[d, u], zr.at[h, lvl, j], up if go_up else down)
 
     def z_valid(go_up, s):
         return ((at - s >= 0) & has_up) if go_up else ((at + s < line) & has_down)
@@ -115,7 +115,7 @@
                 @pl.when((lvl >= 0) & (lvl < line))
                 def _():
                     blk = ws[j % 2].at[h, lvl, p if j < 2 else 1 - p]
-                    remote(blk, blk, zs.at[d, h, s - 1, j], zr.at[d, h, s - 1, j], to_x).wait_recv()
+                    remote(blk, blk, zs.at[d, j % 2], zr.at[h, lvl, j], to_x).wait_recv()
             if s < line - 1:
                 @pl.when(z_valid(go_up, s))
                 def _():
@@ -129,7 +129,7 @@
     for slot, dev in ((1, to_x), (2, to_y)):
         for a in (0, 1):
             first[slot, a] = remote(
-                own[a].at[mine], xs.at[a, slot, mine], ts.at[slot - 1, a], tr.at[slot - 1, a], dev
+                own[a].at[mine], xs.at[a, slot, mine], ts.at[0], tr.at[slot - 1, a], dev
             )
     first[1, 0].start()
     first[2, 1].start()
@@ -139,19 +139,19 @@
     base = pl.multiple_of(core * half, half)
     lead, rest = pl.ds(base, most), pl.ds(base + most, half - most)
     diag = [
-        remote(xs.at[0, 1, lead], xs.at[0, 3, lead], ts.at[2, 0], tr.at[2, 0], to_y),
-        remote(xs.at[1, 2, mine], xs.at[1, 3, mine], ts.at[2, 1], tr.at[2, 1], to_x),
-        remote(xs.at[0, 2, rest], xs.at[0, 3, rest], ts.at[3, 0], tr.at[3, 0], to_x),
+        remote(xs.at[0, 1, lead], xs.at[0, 3, lead], ts.at[0], tr.at[2, 0], to_y),
+        remote(xs.at[1, 2, mine], xs.at[1, 3, mine], ts.at[0], tr.at[2, 1], to_x),
+        remote(xs.at[0, 2, rest], xs.at[0, 3, rest], ts.at[0], tr.at[3, 0], to_x),
     ]
 
     def swap(slot, a):
         return remote(
-            xs.at[a, slot, mine], xs.at[a, slot, mine], cs.at[slot - 1, a], cr.at[slot - 1, a], to_core
+            xs.at[a, slot, mine], xs.at[a, slot, mine], cs.at[0], cr.at[slot - 1, a], to_core
         )
 
     def swapped(slot, a):
         blk = xs.at[a, slot, theirs]
-        remote(blk, blk, cs.at[slot - 1, a], cr.at[slot - 1, a], to_core).wait_recv()
+        remote(blk, blk, cs.at[0], cr.at[slot - 1, a], to_core).wait_recv()
 
     def unit(u, h, slot, lvl):
         if u == 1 and native:
@@ -211,10 +211,14 @@
 
     turns = (1 - p, p)
 
-    def o_copy(go_up, h, o, k):
+    def o_copy(go_up, h, o, k, here=None):
+        def o_last(o):
+            return jnp.where(o == (at - 1 if here is None else at), line, o)
+
         d, b = 0 if go_up else 1, turns[k]
         return remote(
-            dw.at[h, o, b], zin.at[d, h, o, b], os.at[d, h, o, k], orr.at[d, h, o, k], up if go_up else down
+            dw.at[h, o, b], zin.at[d, h, o, b], os.at[d], orr.at[h, o, k] if go_up else orr.at[h, o_last(o), k],
+            up if go_up else down,
         )
 
     def make_dw(h, i):
@@ -245,10 +249,9 @@
 
         lax.fori_loop(0, line, body, 0)
 
-    own_x.wait()
-    own_c.wait()
-    for copy in own_w:
-        copy.wait()
+    both = xs.at[:, 0]
+    pltpu.make_async_copy(both, both, ls.at[0]).wait()
+    pltpu.make_async_copy(fin, fin, ls.at[1]).wait()
 
     def own_level(h):
         for u in (0, 1):
@@ -350,7 +353,7 @@
     def p_copy(slot, k):
         there = lax.rem(c + k, n_tp)
         return remote(
-            part_.at[slot, there], tpin.at[k - 1, slot], ps.at[k - 1, slot], pr.at[k - 1, slot], {"tp": there}
+            part_.at[slot, there], tpin.at[k - 1, slot], ps.at[0], pr.at[k - 1, slot], {"tp": there}
         )
 
     def make_part(slot):
@@ -366,20 +369,35 @@
         for k in range(1, n_tp):
             p_copy(slot, k).start()
 
+    wide = line // 2 * level
+
+    def e_part(slot, k, i):
+        there = lax.rem(c + k, n_tp)
+        span = (pl.ds(0, wide), pl.ds(wide, width - wide))[i]
+        return remote(
+            part_.at[slot, there, :, span], tpin.at[k - 1, slot, :, span],
+            ps.at[0], pr.at[k - 1, 4 * i + slot], {"tp": there},
+        )
+
     def end_part(slot):
-        for k in list(range(1, n_tp)) + [0]:
-            there = lax.rem(c + k, n_tp)
-            tok = pl.ds(pl.multiple_of(there * part, part), part)
-
+        for i, (lo, hi) in enumerate(((0, line // 2), (line // 2, line))):
             def body(lvl, _):
                 span = pl.ds(pl.multiple_of(lvl * level, level), level)
-                value = ahead[there, :, span] + dot(g[1, slot, tok], wu[1, lvl].reshape(level, cols), 1, 1)
-                part_[slot, there, :, span] = value.astype(BF16)
+                value = dot(g[1, slot], wu[1, lvl].reshape(level, cols), 1, 1)
+                part_[slot, :, :, span] = (ahead[:, :, span] + value.reshape(n_tp, part, level)).astype(BF16)
                 return 0
 
-            lax.fori_loop(0, line, body, 0)
-            if k > 0:
-                p_copy(slot, k).start()
+            lax.fori_loop(lo, hi, body, 0)
+            for k in range(1, n_tp):
+                e_part(slot, k, i).start()
+
+    def end_sum(slot, i):
+        span = (pl.ds(0, wide), pl.ds(wide, width - wide))[i]
+        total = part_[slot, c, :, span].astype(F32)
+        for k in range(1, n_tp):
+            e_part(slot, k, i).wait_recv()
+            total = total + tpin[k - 1, slot, :, span].astype(F32)
+        part_[slot, c, :, span] = total.astype(BF16)
 
     def tp_sum(slot):
         for k in range(1, n_tp):
@@ -395,12 +413,12 @@
     left_a, left_b = pl.ds(0, early_cut), pl.ds(early_cut, cut - early_cut)
     q_copies = {
         "x3": remote(part_.at[3, c, :, left], q1.at[1, :, left], qs.at[0], qr.at[0], to_x),
-        "y3": remote(part_.at[3, c, :, right], q1.at[1, :, right], qs.at[1], qr.at[1], to_y),
-        "x1": remote(part_.at[1, c, :, left], q1.at[0, :, left], qs.at[2], qr.at[2], to_x),
-        "y2": remote(part_.at[2, c, :, right], q1.at[0, :, right], qs.at[3], qr.at[3], to_y),
-        "y2a": remote(part_.at[2, c, :, left_a], q2.at[:, left_a], qs.at[4], qr.at[4], to_y),
-        "y2b": remote(part_.at[2, c, :, left_b], q2.at[:, left_b], qs.at[6], qr.at[6], to_y),
-        "x1r": remote(part_.at[1, c, :, right], q2.at[:, right], qs.at[5], qr.at[5], to_x),
+        "y3": remote(part_.at[3, c, :, right], q1.at[1, :, right], qs.at[0], qr.at[1], to_y),
+        "x1": remote(part_.at[1, c, :, left], q1.at[0, :, left], qs.at[0], qr.at[2], to_x),
+        "y2": remote(part_.at[2, c, :, right], q1.at[0, :, right], qs.at[0], qr.at[3], to_y),
+        "y2a": remote(part_.at[2, c, :, left_a], q2.at[:, left_a], qs.at[0], qr.at[4], to_y),
+        "y2b": remote(part_.at[2, c, :, left_b], q2.at[:, left_b], qs.at[0], qr.at[6], to_y),
+        "x1r": remote(part_.at[1, c, :, right], q2.at[:, right], qs.at[0], qr.at[5], to_x),
     }
 
     def store_sum(slot):
@@ -415,7 +433,7 @@
 
             @pl.when((gap > 0) & (gap <= t))
             def _():
-                o_copy(go_up, h, o, k).wait_recv()
+                o_copy(go_up, h, o, k, True).wait_recv()
                 if t < line - 1:
                     dw[h, o, b] = (dw[h, o, b].astype(F32) + zin[d, h, o, b].astype(F32)).astype(BF16)
                     o_copy(go_up, h, o, k).start()
@@ -427,17 +445,17 @@
 
     def e_y(h, i):
         here = dw_at(quarter, h, half_rows[i])
-        return remote(fin.at[h, 1 - p, half_rows[i]], here, es.at[1, h, i], er.at[1, h, i], to_y)
+        return remote(fin.at[h, 1 - p, half_rows[i]], here, es.at[1], er.at[1 + i, h], to_y)
 
     def e_relay(h, i):
         here = dw_at(2 * r + 1 - p, h, half_rows[i])
-        return remote(here, here, es.at[2, h, i], er.at[2, h, i], to_x)
+        return remote(here, here, es.at[2], er.at[3 + i, h], to_x)
 
     def e_x(h):
-        return remote(fin.at[h, p], dw_at(quarter, h), es.at[0, h, 0], er.at[0, h, 0], to_x)
+        return remote(fin.at[h, p], dw_at(quarter, h), es.at[0], er.at[0, h], to_x)
 
     def e_own(h):
-        return pltpu.make_async_copy(fin.at[h, p], dw_at(quarter, h), el.at[h])
+        return pltpu.make_async_copy(fin.at[h, p], dw_at(quarter, h), el.at[0])
 
     def finish(h, k):
         b = turns[k]
@@ -463,7 +481,7 @@
     def relay(h):
         for i in (0, 1):
             blk = dw_at(2 * r + 1 - p, h, half_rows[i])
-            remote(blk, blk, es.at[1, h, i], er.at[1, h, i], to_y).wait_recv()
+            remote(blk, blk, es.at[1], er.at[1 + i, h], to_y).wait_recv()
             e_relay(h, i).start()
 
     def in_x3():
@@ -478,12 +496,12 @@
 
     def out_own(i):
         span = segments[i][0]
-        return pltpu.make_async_copy(fo.at[:, span], din_out.at[c, :, span], dl.at[i])
+        return pltpu.make_async_copy(fo.at[:, span], din_out.at[c, :, span], dl.at[0])
 
     def out_peer(i, k):
         span = segments[i][0]
         return remote(
-            fo.at[:, span], din_out.at[c, :, span], ds.at[k - 1, i], dr.at[k - 1, i], {"tp": lax.rem(c + k, n_tp)}
+            fo.at[:, span], din_out.at[c, :, span], ds.at[0], dr.at[k - 1, i], {"tp": lax.rem(c + k, n_tp)}
         )
 
     def in_last(i):
@@ -530,8 +548,14 @@
         make_part(3)
     for slot in (1, 2, 0):
         last_rows(slot)
-    store_sum(3)
-    send("x3", "y3")
+    if split:
+        end_sum(3, 0)
+        send("x3")
+        end_sum(3, 1)
+        send("y3")
+    else:
+        store_sum(3)
+        send("x3", "y3")
     if split:
         sums(0, 1, 0)
     make_part(1)
@@ -575,50 +599,41 @@
     in_last(2)
 
     for i in range(3):
-        out_own(i).wait()
         for k in range(1, n_tp):
             out_peer(i, k).wait_recv()
-            out_peer(i, k).wait_send()
     for h in range(parts):
         blk = dw_at(2 * (1 - r) + p, h)
-        remote(blk, blk, es.at[0, h, 0], er.at[0, h, 0], to_x).wait_recv()
+        remote(blk, blk, es.at[0], er.at[0, h], to_x).wait_recv()
         for i in (0, 1):
             blk = dw_at(2 * (1 - r) + 1 - p, h, half_rows[i])
-            remote(blk, blk, es.at[2, h, i], er.at[2, h, i], to_x).wait_recv()
-    for copy in q_copies.values():
-        copy.wait_send()
-    for h in range(parts):
-        e_own(h).wait()
-        e_x(h).wait_send()
-        for i in (0, 1):
-            e_y(h, i).wait_send()
-            e_relay(h, i).wait_send()
-    for slot in range(4):
-        for k in range(1, n_tp):
-            p_copy(slot, k).wait_send()
-    for h in range(parts):
-        for o in range(line):
-            @pl.when((at < o) & has_up)
-            def _():
-                for k in (0, 1):
-                    o_copy(True, h, o, k).wait_send()
-
-            @pl.when((at > o) & has_down)
-            def _():
-                for k in (0, 1):
-                    o_copy(False, h, o, k).wait_send()
-    for slot in (1, 2, 3):
-        for a in (0, 1):
-            swap(slot, a).wait_send()
-    for copy in list(first.values()) + diag + y_copies:
-        copy.wait_send()
-    for h in range(parts):
-        for s in range(line - 1):
-            for j in range(4):
-                for go_up in (True, False):
-                    @pl.when(z_valid(go_up, s))
-                    def _():
-                        z_copy(go_up, h, s, j).wait_send()
+            remote(blk, blk, es.at[2], er.at[3 + i, h], to_x).wait_recv()
+
+    def sent(ref, sem):
+        pltpu.make_async_copy(ref, ref, sem).wait()
+
+    sent(fo, dl.at[0])
+    sent(fin.at[:, 0], el.at[0])
+    for i in range(3):
+        sent(fin.at[:, 0], es.at[i])
+    sent(part_.at[pl.ds(0, 3), 0], qs.at[0])
+    if n_tp > 1:
+        sent(tpin, ps.at[0])
+        sent(tpin.at[:, 0], ds.at[0])
+    sent(xs.at[0, pl.ds(0, 3)], ts.at[0])
+    sent(xs.at[0, pl.ds(0, 3)], cs.at[0])
+    sent(fin, ys.at[0])
+    for k in range(line):
+        @pl.when((at == k) & has_up)
+        def _():
+            sent(dw.at[:, pl.ds(0, max(line - 1 - k, 1))], os.at[0])
+            for u in (0, 1):
+                sent(ws[u].at[:, pl.ds(0, k + 1)], zs.at[0, u])
+
+        @pl.when((at == k) & has_down)
+        def _():
+            sent(dw.at[:, pl.ds(0, max(k, 1))], os.at[1])
+            for u in (0, 1):
+                sent(ws[u].at[:, pl.ds(0, line - k)], zs.at[1, u])
 
 
 def fused(n_fs, n_tp, n_rep, x, c, w_up, w_down):
@@ -660,12 +675,12 @@
             vmem(part, width),
             vmem(part, width),
             pltpu.VMEM((n_tp, part, width) if parts > 1 else (1, 8, 128), F32),
-            dma((2, parts, line, 4)), dma((2, parts, line, 4)), dma((parts, 2)), dma((parts, 2)),
-            dma((4, 2)), dma((4, 2)), dma((3, 2)), dma((3, 2)), dma((2 + 2 * parts,)),
-            dma((2, parts, line, 2)), dma((2, parts, line, 2)),
-            dma((4, parts, 2)), dma((4, parts, 2)), dma((parts,)),
-            dma((others, 4)), dma((others, 4)), dma((7,)), dma((7,)),
-            dma((others, 3)), dma((others, 3)), dma((3,)),
+            dma((2, 2)), dma((parts, line, 4)), dma((1,)), dma((parts, 2)),
+            dma((1,)), dma((4, 2)), dma((1,)), dma((3, 2)), dma((2,)),
+            dma((2,)), dma((parts, line + 1, 2)),
+            dma((3,)), dma((5, parts)), dma((1,)),
+            dma((1,)), dma((others, 8)), dma((1,)), dma((7,)),
+            dma((1,)), dma((others, 3)), dma((1,)),
         ],
         compiler_params=pltpu.CompilerParams(
             collective_id=0, has_side_effects=True, vmem_limit_bytes=52 * 2**20

time: 120 us -> 118 us (0.983)
  Pallas kernels: 117 us -> 114 us
    pallas_call x1, Pallas kernels: 117 us -> 114 us  [fused(): pl.pallas_call(functools.partial(kernel, line, n_tp, native, parts), out_...]
where the time goes in v5:
time: 118 us
  Pallas kernels  114 us (97%)
  other arithmetic  1.57 us (1%)
  local copies, waits for them, and re-layouts  1.47 us (1%)
    pallas_call x1, Pallas kernels, fused(): pl.pallas_call(functools.partial(kernel, line, n_tp, native, parts), out_...  114 us

profile of v5, /device:TPU:0, one launch (start us, length us, event | category | flops | bytes accessed | tf_op | source)
XLA Modules:
  0.0 117.7 jit_solution(11428230810357585606)
XLA Ops:
  0.6 114.0 %fused.1 = (bf16[256,2048]{1,0:T(8,128)(2,1)S(1)}, bf16[2,192,2048]{2,1,0:T(8,128)(2,1)}) custom-call(bf16[384,2048]{1,0:T(8,128)(2,1)} %x_in.1, bf16[384,2048]{1,0:T(8,128)(2,1)} %c_in.1, bf16[256,2048]{1,0:T(8,128)(2,1)} %up_in.1, bf16[2048,256]{1,0:T(8,128)(2,1)} %down_in.1), custom_call_target="tpu_custom_call" | custom-call | tf_op jit(solution)/shard_map/fused/pallas_call | solution.py:655
  114.6 0.0 copy-start
  114.6 1.6 %convert_element_type.3 = f32[256,2048]{1,0:T(8,128)} convert(bf16[256,2048]{1,0:T(8,128)(2,1)S(1)} %get-tuple-element.5) | non-fusion elementwise | flops 524288 | bytes 3145728 | tf_op jit(solution)/shard_map/convert_element_type | solution.py:695
  116.2 0.3 copy-done
  116.5 1.1 copy.7
Async XLA Ops:
  114.6 1.9 %copy-start = (bf16[2,192,2048]{2,1,0:T(8,128)(2,1)S(1)}, bf16[2,192,2048]{2,1,0:T(8,128)(2,1)}, u32[]{:S(2)}) copy-start(bf16[2,192,2048]{2,1,0:T(8,128)(2,1)} %get-tuple-element.4) | copy-start | bytes 4718596

commit v6 on v5

--- a/solution.py
+++ b/solution.py
@@ -369,35 +369,39 @@
         for k in range(1, n_tp):
             p_copy(slot, k).start()
 
-    wide = line // 2 * level
+    marks = [i * line // 4 for i in range(5)]
+    turn = (2, 0, 1, 3)
+
+    def group(i):
+        return pl.ds(marks[i] * level, (marks[i + 1] - marks[i]) * level)
 
     def e_part(slot, k, i):
         there = lax.rem(c + k, n_tp)
-        span = (pl.ds(0, wide), pl.ds(wide, width - wide))[i]
         return remote(
-            part_.at[slot, there, :, span], tpin.at[k - 1, slot, :, span],
+            part_.at[slot, there, :, group(i)], tpin.at[k - 1, slot, :, group(i)],
             ps.at[0], pr.at[k - 1, 4 * i + slot], {"tp": there},
         )
 
     def end_part(slot):
-        for i, (lo, hi) in enumerate(((0, line // 2), (line // 2, line))):
+        for i in turn:
             def body(lvl, _):
                 span = pl.ds(pl.multiple_of(lvl * level, level), level)
                 value = dot(g[1, slot], wu[1, lvl].reshape(level, cols), 1, 1)
                 part_[slot, :, :, span] = (ahead[:, :, span] + value.reshape(n_tp, part, level)).astype(BF16)
                 return 0
 
-            lax.fori_loop(lo, hi, body, 0)
+            lax.fori_loop(marks[i], marks[i + 1], body, 0)
             for k in range(1, n_tp):
                 e_part(slot, k, i).start()
 
     def end_sum(slot, i):
-        span = (pl.ds(0, wide), pl.ds(wide, width - wide))[i]
-        total = part_[slot, c, :, span].astype(F32)
+        total = part_[slot, c, :, group(i)].astype(F32)
         for k in range(1, n_tp):
             e_part(slot, k, i).wait_recv()
-            total = total + tpin[k - 1, slot, :, span].astype(F32)
-        part_[slot, c, :, span] = total.astype(BF16)
+            total = total + tpin[k - 1, slot, :, group(i)].astype(F32)
+        part_[slot, c, :, group(i)] = total.astype(BF16)
+        for copy in third[i]:
+            copy.start()
 
     def tp_sum(slot):
         for k in range(1, n_tp):
@@ -408,12 +412,23 @@
         return total
 
     cut = width * 3 // 8 // 128 * 128
-    early_cut = cut // 256 * 128
+    early_cut = cut * 2 // 384 * 128
     left, right = pl.ds(0, cut), pl.ds(cut, width - cut)
     left_a, left_b = pl.ds(0, early_cut), pl.ds(early_cut, cut - early_cut)
+    third = []
+    for i in range(4):
+        lo, hi = marks[i] * level, marks[i + 1] * level
+        mid = min(max(cut, lo), hi)
+        third.append([])
+        for k, (start, stop, dev) in enumerate(((lo, mid, to_x), (mid, hi, to_y))):
+            if stop > start:
+                span = pl.ds(start, stop - start)
+                third[i].append(
+                    remote(part_.at[3, c, :, span], q1.at[1, :, span], qs.at[0], qr.at[8 + 2 * i + k], dev)
+                )
+    toward_x = [third[i][0] for i in range(4) if marks[i] * level < cut]
+    toward_y = [third[i][-1] for i in range(4) if marks[i + 1] * level > cut]
     q_copies = {
-        "x3": remote(part_.at[3, c, :, left], q1.at[1, :, left], qs.at[0], qr.at[0], to_x),
-        "y3": remote(part_.at[3, c, :, right], q1.at[1, :, right], qs.at[0], qr.at[1], to_y),
         "x1": remote(part_.at[1, c, :, left], q1.at[0, :, left], qs.at[0], qr.at[2], to_x),
         "y2": remote(part_.at[2, c, :, right], q1.at[0, :, right], qs.at[0], qr.at[3], to_y),
         "y2a": remote(part_.at[2, c, :, left_a], q2.at[:, left_a], qs.at[0], qr.at[4], to_y),
@@ -485,11 +500,13 @@
             e_relay(h, i).start()
 
     def in_x3():
-        q_copies["x3"].wait_recv()
+        for copy in toward_x:
+            copy.wait_recv()
         part_[2, c, :, left] = (part_[2, c, :, left].astype(F32) + q1[1, :, left].astype(F32)).astype(BF16)
 
     def in_y3():
-        q_copies["y3"].wait_recv()
+        for copy in toward_y:
+            copy.wait_recv()
         part_[1, c, :, right] = (part_[1, c, :, right].astype(F32) + q1[1, :, right].astype(F32)).astype(BF16)
 
     segments = ((right, ("y2", "x1r")), (left_a, ("x1", "y2a")), (left_b, ("y2b",)))
@@ -533,12 +550,9 @@
         for i in range(lo, min(hi, line)):
             make_dw(final, i)
 
-    def close(h):
-        for k in (0, 1):
-            sums(h, line - 1, k)
-            finish(h, k)
-            if (h, k) == (final, 0):
-                send("y2b")
+    def close(h, k):
+        sums(h, line - 1, k)
+        finish(h, k)
 
     split = parts > 1
     last_rows(3)
@@ -546,16 +560,20 @@
         end_part(3)
     else:
         make_part(3)
-    for slot in (1, 2, 0):
-        last_rows(slot)
-    if split:
+    last_rows(1)
+    if split:
+        end_sum(3, 2)
         end_sum(3, 0)
-        send("x3")
+    last_rows(2)
+    if split:
         end_sum(3, 1)
-        send("y3")
-    else:
+        end_sum(3, 3)
+    last_rows(0)
+    if not split:
         store_sum(3)
-        send("x3", "y3")
+        for copies in third:
+            for copy in copies:
+                copy.start()
     if split:
         sums(0, 1, 0)
     make_part(1)
@@ -578,24 +596,25 @@
         for k in (0, 1):
             sums(0, t, k)
     if split:
-        close(0)
+        close(0, 0)
+        close(0, 1)
     in_x3()
-    send("y2a")
     in_y3()
     send("x1r")
-    if not split:
-        close(0)
     for h in range(1, parts):
         for t in range(1, line - 1):
             for k in (0, 1):
                 sums(h, t, k)
-        relay(h - 1)
-        close(h)
+    close(final, 0)
+    send("y2a", "y2b")
+    if split:
+        relay(0)
+    close(final, 1)
     for k in range(1, n_tp):
         p_copy(0, k).wait_recv()
     in_last(0)
+    relay(final)
     in_last(1)
-    relay(final)
     in_last(2)
 
     for i in range(3):
@@ -641,7 +660,7 @@
     tokens, width = x.shape
     rows, block = w_up.shape
     cols = block // (2 * n_rep)
-    parts = 2 if cols % 256 == 0 and n_fs > 4 else 1
+    parts = 2 if cols % 256 == 0 and n_fs >= 8 else 1
     cols = cols // parts
     native = rows % 128 == 0
     if not native:
@@ -679,7 +698,7 @@
             dma((1,)), dma((4, 2)), dma((1,)), dma((3, 2)), dma((2,)),
             dma((2,)), dma((parts, line + 1, 2)),
             dma((3,)), dma((5, parts)), dma((1,)),
-            dma((1,)), dma((others, 8)), dma((1,)), dma((7,)),
+            dma((1,)), dma((others, 16)), dma((1,)), dma((16,)),
             dma((1,)), dma((others, 3)), dma((1,)),
         ],
         compiler_params=pltpu.CompilerParams(

time: 118 us -> 117 us (level)
  no operation moved by 1% of the time
where the time goes in v6:
time: 117 us
  Pallas kernels  113 us (97%)
  other arithmetic  1.57 us (1%)
  local copies, waits for them, and re-layouts  1.47 us (1%)
    pallas_call x1, Pallas kernels, fused(): pl.pallas_call(functools.partial(kernel, line, n_tp, native, parts), out_...  113 us

profile of v6, /device:TPU:0, one launch (start us, length us, event | category | flops | bytes accessed | tf_op | source)
XLA Modules:
  0.0 117.1 jit_solution(6211299435619543688)
XLA Ops:
  0.6 113.4 %fused.1 = (bf16[256,2048]{1,0:T(8,128)(2,1)S(1)}, bf16[2,192,2048]{2,1,0:T(8,128)(2,1)}) custom-call(bf16[384,2048]{1,0:T(8,128)(2,1)} %x_in.1, bf16[384,2048]{1,0:T(8,128)(2,1)} %c_in.1, bf16[256,2048]{1,0:T(8,128)(2,1)} %up_in.1, bf16[2048,256]{1,0:T(8,128)(2,1)} %down_in.1), custom_call_target="tpu_custom_call" | custom-call | tf_op jit(solution)/shard_map/fused/pallas_call | solution.py:674
  114.0 0.0 copy-start
  114.0 1.6 %convert_element_type.3 = f32[256,2048]{1,0:T(8,128)} convert(bf16[256,2048]{1,0:T(8,128)(2,1)S(1)} %get-tuple-element.5) | non-fusion elementwise | flops 524288 | bytes 3145728 | tf_op jit(solution)/shard_map/convert_element_type | solution.py:714
  115.6 0.3 copy-done
  115.9 1.1 copy.7
Async XLA Ops:
  114.0 1.9 %copy-start = (bf16[2,192,2048]{2,1,0:T(8,128)(2,1)S(1)}, bf16[2,192,2048]{2,1,0:T(8,128)(2,1)}, u32[]{:S(2)}) copy-start(bf16[2,192,2048]{2,1,0:T(8,128)(2,1)} %get-tuple-element.4) | copy-start | bytes 4718596

commit v7 on v6

--- a/solution.py
+++ b/solution.py
@@ -379,7 +379,7 @@
         there = lax.rem(c + k, n_tp)
         return remote(
             part_.at[slot, there, :, group(i)], tpin.at[k - 1, slot, :, group(i)],
-            ps.at[0], pr.at[k - 1, 4 * i + slot], {"tp": there},
+            ps.at[0], pr.at[k - 1, 3 + i], {"tp": there},
         )
 
     def end_part(slot):
@@ -424,7 +424,7 @@
             if stop > start:
                 span = pl.ds(start, stop - start)
                 third[i].append(
-                    remote(part_.at[3, c, :, span], q1.at[1, :, span], qs.at[0], qr.at[8 + 2 * i + k], dev)
+                    remote(part_.at[3, c, :, span], q1.at[1, :, span], qs.at[0], qr.at[7 + i if k == 0 else 11 + i], dev)
                 )
     toward_x = [third[i][0] for i in range(4) if marks[i] * level < cut]
     toward_y = [third[i][-1] for i in range(4) if marks[i + 1] * level > cut]
@@ -560,10 +560,10 @@
         end_part(3)
     else:
         make_part(3)
-    last_rows(1)
     if split:
         end_sum(3, 2)
         end_sum(3, 0)
+    last_rows(1)
     last_rows(2)
     if split:
         end_sum(3, 1)
@@ -698,7 +698,7 @@
             dma((1,)), dma((4, 2)), dma((1,)), dma((3, 2)), dma((2,)),
             dma((2,)), dma((parts, line + 1, 2)),
             dma((3,)), dma((5, parts)), dma((1,)),
-            dma((1,)), dma((others, 16)), dma((1,)), dma((16,)),
+            dma((1,)), dma((others, 7)), dma((1,)), dma((16,)),
             dma((1,)), dma((others, 3)), dma((1,)),
         ],
         compiler_params=pltpu.CompilerParams(

time: 117 us -> 117 us (level)
  no operation moved by 1% of the time
where the time goes in v7:
time: 117 us
  Pallas kernels  113 us (97%)
  other arithmetic  1.57 us (1%)
  local copies, waits for them, and re-layouts  1.47 us (1%)
    pallas_call x1, Pallas kernels, fused(): pl.pallas_call(functools.partial(kernel, line, n_tp, native, parts), out_...  113 us

profile of v7, /device:TPU:0, one launch (start us, length us, event | category | flops | bytes accessed | tf_op | source)
XLA Modules:
  0.0 116.7 jit_solution(4882805875751394830)
XLA Ops:
  0.6 113.1 %fused.1 = (bf16[256,2048]{1,0:T(8,128)(2,1)S(1)}, bf16[2,192,2048]{2,1,0:T(8,128)(2,1)}) custom-call(bf16[384,2048]{1,0:T(8,128)(2,1)} %x_in.1, bf16[384,2048]{1,0:T(8,128)(2,1)} %c_in.1, bf16[256,2048]{1,0:T(8,128)(2,1)} %up_in.1, bf16[2048,256]{1,0:T(8,128)(2,1)} %down_in.1), custom_call_target="tpu_custom_call" | custom-call | tf_op jit(solution)/shard_map/fused/pallas_call | solution.py:674
  113.7 0.0 copy-start
  113.7 1.6 %convert_element_type.3 = f32[256,2048]{1,0:T(8,128)} convert(bf16[256,2048]{1,0:T(8,128)(2,1)S(1)} %get-tuple-element.5) | non-fusion elementwise | flops 524288 | bytes 3145728 | tf_op jit(solution)/shard_map/convert_element_type | solution.py:714
  115.3 0.3 copy-done
  115.6 1.1 copy.7
Async XLA Ops:
  113.7 1.9 %copy-start = (bf16[2,192,2048]{2,1,0:T(8,128)(2,1)S(1)}, bf16[2,192,2048]{2,1,0:T(8,128)(2,1)}, u32[]{:S(2)}) copy-start(bf16[2,192,2048]{2,1,0:T(8,128)(2,1)} %get-tuple-element.4) | copy-start | bytes 4718596

commit v8 on v7

--- a/solution.py
+++ b/solution.py
@@ -412,7 +412,7 @@
         return total
 
     cut = width * 3 // 8 // 128 * 128
-    early_cut = cut * 2 // 384 * 128
+    early_cut = max(cut - 128, 128)
     left, right = pl.ds(0, cut), pl.ds(cut, width - cut)
     left_a, left_b = pl.ds(0, early_cut), pl.ds(early_cut, cut - early_cut)
     third = []
@@ -614,6 +614,28 @@
         p_copy(0, k).wait_recv()
     in_last(0)
     relay(final)
+
+    def sent(ref, sem):
+        pltpu.make_async_copy(ref, ref, sem).wait()
+
+    if n_tp > 1:
+        sent(tpin, ps.at[0])
+    sent(xs.at[0, pl.ds(0, 3)], ts.at[0])
+    sent(xs.at[0, pl.ds(0, 3)], cs.at[0])
+    sent(fin, ys.at[0])
+    for k in range(line):
+        @pl.when((at == k) & has_up)
+        def _():
+            sent(dw.at[:, pl.ds(0, max(line - 1 - k, 1))], os.at[0])
+            for u in (0, 1):
+                sent(ws[u].at[:, pl.ds(0, k + 1)], zs.at[0, u])
+
+        @pl.when((at == k) & has_down)
+        def _():
+            sent(dw.at[:, pl.ds(0, max(k, 1))], os.at[1])
+            for u in (0, 1):
+                sent(ws[u].at[:, pl.ds(0, line - k)], zs.at[1, u])
+
     in_last(1)
     in_last(2)
 
@@ -627,32 +649,13 @@
             blk = dw_at(2 * (1 - r) + 1 - p, h, half_rows[i])
             remote(blk, blk, es.at[2], er.at[3 + i, h], to_x).wait_recv()
 
-    def sent(ref, sem):
-        pltpu.make_async_copy(ref, ref, sem).wait()
-
     sent(fo, dl.at[0])
     sent(fin.at[:, 0], el.at[0])
     for i in range(3):
         sent(fin.at[:, 0], es.at[i])
     sent(part_.at[pl.ds(0, 3), 0], qs.at[0])
     if n_tp > 1:
-        sent(tpin, ps.at[0])
         sent(tpin.at[:, 0], ds.at[0])
-    sent(xs.at[0, pl.ds(0, 3)], ts.at[0])
-    sent(xs.at[0, pl.ds(0, 3)], cs.at[0])
-    sent(fin, ys.at[0])
-    for k in range(line):
-        @pl.when((at == k) & has_up)
-        def _():
-            sent(dw.at[:, pl.ds(0, max(line - 1 - k, 1))], os.at[0])
-            for u in (0, 1):
-                sent(ws[u].at[:, pl.ds(0, k + 1)], zs.at[0, u])
-
-        @pl.when((at == k) & has_down)
-        def _():
-            sent(dw.at[:, pl.ds(0, max(k, 1))], os.at[1])
-            for u in (0, 1):
-                sent(ws[u].at[:, pl.ds(0, line - k)], zs.at[1, u])
 
 
 def fused(n_fs, n_tp, n_rep, x, c, w_up, w_down):

time: 117 us -> 117 us (level)
  no operation moved by 1% of the time
where the time goes in v8:
time: 117 us
  Pallas kernels  113 us (97%)
  other arithmetic  1.57 us (1%)
  local copies, waits for them, and re-layouts  1.47 us (1%)
    pallas_call x1, Pallas kernels, fused(): pl.pallas_call(functools.partial(kernel, line, n_tp, native, parts), out_...  113 us

profile of v8, /device:TPU:0, one launch (start us, length us, event | category | flops | bytes accessed | tf_op | source)
XLA Modules:
  0.0 116.7 jit_solution(10706413784798312850)
XLA Ops:
  0.6 113.0 %fused.1 = (bf16[256,2048]{1,0:T(8,128)(2,1)S(1)}, bf16[2,192,2048]{2,1,0:T(8,128)(2,1)}) custom-call(bf16[384,2048]{1,0:T(8,128)(2,1)} %x_in.1, bf16[384,2048]{1,0:T(8,128)(2,1)} %c_in.1, bf16[256,2048]{1,0:T(8,128)(2,1)} %up_in.1, bf16[2048,256]{1,0:T(8,128)(2,1)} %down_in.1), custom_call_target="tpu_custom_call" | custom-call | tf_op jit(solution)/shard_map/fused/pallas_call | solution.py:677
  113.7 0.0 copy-start
  113.7 1.6 %convert_element_type.3 = f32[256,2048]{1,0:T(8,128)} convert(bf16[256,2048]{1,0:T(8,128)(2,1)S(1)} %get-tuple-element.5) | non-fusion elementwise | flops 524288 | bytes 3145728 | tf_op jit(solution)/shard_map/convert_element_type | solution.py:717
  115.2 0.3 copy-done
  115.6 1.1 copy.7
Async XLA Ops:
  113.7 1.9 %copy-start = (bf16[2,192,2048]{2,1,0:T(8,128)(2,1)S(1)}, bf16[2,192,2048]{2,1,0:T(8,128)(2,1)}, u32[]{:S(2)}) copy-start(bf16[2,192,2048]{2,1,0:T(8,128)(2,1)} %get-tuple-element.4) | copy-start | bytes 4718596
